TPU v7x, 512 devices: a whole 4x4x16 slice. The times are simulated.
512 devices in a mesh: sp: 256 (over z, y, x), tp: 2 (over core).
Axes of the slice: x: 4, y: 4, z: 16, core: 2. Of those that a mesh axis runs over, the one named last changes fastest.
Arguments:
- stream: bfloat16 [1024, 131072], P('tp', 'sp'), may hold values from -6 to 6
- norm_gain: float32 [2, 1024], replicated, may hold values from 0.1 to 1.9
- w_value: bfloat16 [2, 512, 1024], P(None, 'tp'), may hold values from -0.1875 to 0.1875
- w_gate: bfloat16 [2, 512, 1024], P(None, 'tp'), may hold values from -0.1875 to 0.1875
- conv_taps: bfloat16 [2, 512, 255], P(None, 'tp'), may hold values from -0.375 to 0.375
- group_gain: float32 [2, 512], P(None, 'tp'), may hold values from 0.1 to 1.9
- group_shift: float32 [2, 512], P(None, 'tp'), may hold values from -3 to 3
- w_out: bfloat16 [2, 1024, 512], P(None, 'tp'), may hold values from -0.25 to 0.25
Outputs:
- result: bfloat16 [1024, 131072], P('tp', 'sp')
All inputs are finite; a program needn't handle non-finite values.
Results may differ from a plain program's by a relative error of at most 0.014.
Values may be sent and summed in bfloat16 or wider, within the bound.
No kernel may reach another device: no remote copies, remote signals or barrier semaphores. Data moves between devices by JAX's collectives and lax.ppermute only.
A program may use at most 64 MiB of HBM per device.

v0:
```python
import jax
import jax.numpy as jnp
from jax import lax
from jax.sharding import PartitionSpec as P

GROUP_DIM = 128


RMS_EPS = 1e-06
LN_EPS = 1e-05


def in_order(parts, dim):
    parts = jnp.moveaxis(parts, 0, dim)
    shape = parts.shape
    return parts.reshape(*shape[:dim], shape[dim] * shape[dim + 1], *shape[dim + 2 :])


def sent_to_all(value, axis):
    count = lax.axis_size(axis)
    return lax.all_to_all(
        jnp.broadcast_to(value[None], (count, *value.shape)), axis, 0, 0, tiled=True
    )


def gathered_copies(value, axis, dim):
    return in_order(sent_to_all(value, axis), dim)


def with_halo(cells, sides, width):
    for axis, dim in sides:
        count = lax.axis_size(axis)
        ends = count - 1
        head = lax.slice_in_dim(cells, 0, width, axis=dim)
        tail = lax.slice_in_dim(cells, cells.shape[dim] - width, cells.shape[dim], axis=dim)
        cells = jnp.concatenate(
            [
                lax.ppermute(tail, axis, [(i, (i + 1) % count) for i in range(ends)]),
                cells,
                lax.ppermute(head, axis, [((i + 1) % count, i) for i in range(ends)]),
            ],
            axis=dim,
        )
    return cells


def make_gated(whole, gain, value_weight, gate_weight):
    widened = whole.astype(jnp.float32)
    inverse_rms = lax.rsqrt(jnp.mean(widened * widened, axis=0, keepdims=True) + RMS_EPS)
    normed = (widened * inverse_rms * gain[:, None]).astype(jnp.bfloat16)
    projected = jnp.dot(value_weight, normed, preferred_element_type=jnp.float32).astype(
        jnp.bfloat16
    )
    gate_proj = jnp.dot(gate_weight, normed, preferred_element_type=jnp.float32).astype(
        jnp.bfloat16
    )
    return (projected.astype(jnp.float32) * jax.nn.sigmoid(gate_proj.astype(jnp.float32))).astype(
        jnp.bfloat16
    )


def filter_norm(padded, taps, ggain, gshift):
    channels = taps.shape[0]
    filtered = lax.conv_general_dilated(
        padded[None],
        taps[:, None, :],
        (1,),
        [(0, 0)],
        dimension_numbers=("NCW", "OIW", "NCW"),
        feature_group_count=channels,
        preferred_element_type=jnp.float32,
    )[0]
    tokens_here = filtered.shape[1]
    grouped = filtered.reshape(channels // GROUP_DIM, GROUP_DIM, tokens_here)
    group_mean = jnp.mean(grouped, axis=1, keepdims=True)
    centred = grouped - group_mean
    scaled = centred * lax.rsqrt(jnp.mean(centred * centred, axis=1, keepdims=True) + LN_EPS)
    scaled = scaled.reshape(channels, tokens_here) * ggain[:, None] + gshift[:, None]
    return jax.nn.silu(scaled).astype(jnp.bfloat16)


def body(stream, norm_gain, w_value, w_gate, conv_taps, group_gain, group_shift, w_out):
    rim_width = (conv_taps.shape[2] - 1) // 2
    layers = w_value.shape[0]
    for layer_index in range(layers):
        whole = gathered_copies(stream, "tp", 0)
        gated = make_gated(whole, norm_gain[layer_index], w_value[layer_index], w_gate[layer_index])
        padded = with_halo(gated, (("sp", 1),), rim_width)
        activated = filter_norm(
            padded, conv_taps[layer_index], group_gain[layer_index], group_shift[layer_index]
        )
        out_weight = w_out[layer_index]
        initial = jnp.zeros((out_weight.shape[0], activated.shape[1]), jnp.float32)
        branch = initial + jnp.dot(
            out_weight, gathered_copies(activated, "tp", 0), preferred_element_type=jnp.float32
        )
        stream = (stream.astype(jnp.float32) + branch).astype(jnp.bfloat16)
    return stream


def solution(mesh):
    placed = (
        P("tp", "sp"),
        P(),
        P(None, "tp", None),
        P(None, "tp", None),
        P(None, "tp", None),
        P(None, "tp"),
        P(None, "tp"),
        P(None, "tp", None),
    )
    return jax.shard_map(body, mesh=mesh, in_specs=placed, out_specs=P("tp", "sp"), check_vma=False)
```

profile of v0, /device:TPU:385, one launch (start us, length us, event | category | flops | bytes accessed | tf_op | source)
XLA Modules:
  0.0 111.9 jit_solution(7844882692543539370)
XLA Ops:
  0.0 2.1 %broadcast_in_dim.16 = bf16[2,512,512]{2,1,0:T(8,128)(2,1)} broadcast(bf16[512,512]{1,0:T(8,128)(2,1)} %param.8), dimensions={1,2} | broadcast | bytes 1572864 | tf_op jit(solution)/shard_map/broadcast_in_dim | solution.py:22
  2.1 4.4 %all-to-all-start = ((bf16[2,512,512]{2,1,0:T(8,128)(2,1)}), bf16[2,512,512]{2,1,0:T(8,128)(2,1)S(1)}, u32[]{:S(2)}, u32[]{:S(2)}) async-start(bf16[2,512,512]{2,1,0:T(8,128)(2,1)} %broadcast_in_dim.16), calls=%async_computation | async-start | bytes 2097152 | tf_op jit(solution)/shard_map/all_to_all | solution.py:21
  6.5 1.7 %all-to-all-done = bf16[2,512,512]{2,1,0:T(8,128)(2,1)S(1)} async-done(((bf16[2,512,512]{2,1,0:T(8,128)(2,1)}), bf16[2,512,512]{2,1,0:T(8,128)(2,1)S(1)}, u32[]{:S(2)}, u32[]{:S(2)}) %all-to-all-start) | async-done | bytes 1048608 | tf_op jit(solution)/shard_map/all_to_all | solution.py:21
  8.8 0.9 copy-done.5
  10.2 0.7 copy-done.7
  11.5 8.6 %collective-permute-start.1 = (bf16[256,127]{0,1:T(8,128)(2,1)S(1)}, bf16[256,127]{0,1:T(8,128)(2,1)S(1)}, u32[]{:S(2)}, u32[]{:S(2)}) collective-permute-start(bf16[256,127]{0,1:T(8,128)(2,1)S(1)} %get-tuple-element.10), channel_id=1, source_target_pairs={{2,0},{4,2},{6,4},{8,6},{10,8},{12,10},{14,12},{16,14},{18,16},{20... | collective-permute-start | bytes 195080 | tf_op jit(solution)/shard_map/ppermute | solution.py:40
  20.2 1.9 %collective-permute-start = (bf16[256,127]{0,1:T(8,128)(2,1)S(1)}, bf16[256,127]{0,1:T(8,128)(2,1)S(1)}, u32[]{:S(2)}, u32[]{:S(2)}) collective-permute-start(bf16[256,127]{0,1:T(8,128)(2,1)S(1)} %get-tuple-element.9), channel_id=1, source_target_pairs={{0,2},{2,4},{4,6},{6,8},{8,10},{10,12},{12,14},{14,16},{16,18},{18... | collective-permute-start | bytes 195080 | tf_op jit(solution)/shard_map/ppermute | solution.py:38
  23.1 7.5 %collective-permute-done = bf16[256,127]{0,1:T(8,128)(2,1)S(1)} collective-permute-done((bf16[256,127]{0,1:T(8,128)(2,1)S(1)}, bf16[256,127]{0,1:T(8,128)(2,1)S(1)}, u32[]{:S(2)}, u32[]{:S(2)}) %collective-permute-start) | collective-permute-done | bytes 65056 | tf_op jit(solution)/shard_map/ppermute | solution.py:38
  30.7 20.1 %fusion.30 = f32[1,256,512]{1,0,2:T(1,128)S(1)} fusion(bf16[256,1,255]{0,1,2:T(2,128)(2,1)S(1)} %copy.56, bf16[1,256,766]{1,2,0:T(8,128)(2,1)S(1)} %maximum_bitcast_fusion), kind=kOutput, calls=%fused_computation.40 | convolution fusion | flops 66846720 | bytes 1047040 | tf_op jit(solution)/shard_map/conv_general_dilated | solution.py:64
  50.8 0.7 copy.58
  51.4 0.6 reduce_sum.55
  52.1 1.6 %multiply_reduce_fusion.1 = f32[2,512]{0,1:T(8,128)S(1)} fusion(f32[2,128,512]{1,0,2:T(2,128)S(1)} %bitcast.105, f32[2,512]{0,1:T(8,128)S(1)} %broadcast_multiply_fusion.1), kind=kLoop, calls=%fused_computation.63 | loop fusion | flops 392192 | bytes 532480 | tf_op jit(solution)/shard_map/reduce_sum | solution.py:77
  54.4 5.7 %all_to_all.20 = bf16[2,256,512]{2,1,0:T(8,128)(2,1)S(1)} all-to-all(bf16[2,256,512]{2,1,0:T(8,128)(2,1)S(1)} %broadcast_in_dim.19), channel_id=1, replica_groups=mesh['sp'=256,'tp'=2] {'tp'}, dimensions={0} | all-to-all | bytes 1048576 | tf_op jit(solution)/shard_map/all_to_all | solution.py:21
  60.9 4.6 %all_to_all.21 = bf16[2,512,512]{2,1,0:T(8,128)(2,1)S(1)} all-to-all(bf16[2,512,512]{2,1,0:T(8,128)(2,1)S(1)} %broadcast_in_dim.20), channel_id=1, replica_groups=mesh['sp'=256,'tp'=2] {'tp'}, dimensions={0} | all-to-all | bytes 2097152 | tf_op jit(solution)/shard_map/all_to_all | solution.py:21
  66.2 0.9 copy-done.6
  67.6 0.7 copy-done.8
  68.9 1.9 %collective-permute-start.3 = (bf16[256,127]{0,1:T(8,128)(2,1)S(1)}, bf16[256,127]{0,1:T(8,128)(2,1)S(1)}, u32[]{:S(2)}, u32[]{:S(2)}) collective-permute-start(bf16[256,127]{0,1:T(8,128)(2,1)S(1)} %get-tuple-element.8), channel_id=1, source_target_pairs={{2,0},{4,2},{6,4},{8,6},{10,8},{12,10},{14,12},{16,14},{18,16},{20... | collective-permute-start | bytes 195080 | tf_op jit(solution)/shard_map/ppermute | solution.py:40
  70.8 3.4 %collective-permute-start.2 = (bf16[256,127]{0,1:T(8,128)(2,1)S(1)}, bf16[256,127]{0,1:T(8,128)(2,1)S(1)}, u32[]{:S(2)}, u32[]{:S(2)}) collective-permute-start(bf16[256,127]{0,1:T(8,128)(2,1)S(1)} %get-tuple-element.7), channel_id=1, source_target_pairs={{0,2},{2,4},{4,6},{6,8},{8,10},{10,12},{12,14},{14,16},{16,18},{18... | collective-permute-start | bytes 195080 | tf_op jit(solution)/shard_map/ppermute | solution.py:38
  74.5 6.7 %collective-permute-done.2 = bf16[256,127]{0,1:T(8,128)(2,1)S(1)} collective-permute-done((bf16[256,127]{0,1:T(8,128)(2,1)S(1)}, bf16[256,127]{0,1:T(8,128)(2,1)S(1)}, u32[]{:S(2)}, u32[]{:S(2)}) %collective-permute-start.2) | collective-permute-done | bytes 65056 | tf_op jit(solution)/shard_map/ppermute | solution.py:38
  81.3 20.1 %fusion.28 = f32[1,256,512]{1,0,2:T(1,128)S(1)} fusion(bf16[256,1,255]{0,1,2:T(2,128)(2,1)S(1)} %copy.63, bf16[1,256,766]{1,2,0:T(8,128)(2,1)S(1)} %maximum_bitcast_fusion.1), kind=kOutput, calls=%fused_computation.38 | convolution fusion | flops 66846720 | bytes 1047040 | tf_op jit(solution)/shard_map/conv_general_dilated | solution.py:64
  101.4 0.7 copy.65
  102.7 1.6 %multiply_reduce_fusion = f32[2,512]{0,1:T(8,128)S(1)} fusion(f32[2,128,512]{1,0,2:T(2,128)S(1)} %bitcast.103, f32[2,512]{0,1:T(8,128)S(1)} %broadcast_multiply_fusion), kind=kLoop, calls=%fused_computation.58 | loop fusion | flops 392192 | bytes 532480 | tf_op jit(solution)/shard_map/reduce_sum | solution.py:77
  105.0 5.4 %all_to_all.22 = bf16[2,256,512]{2,1,0:T(8,128)(2,1)S(1)} all-to-all(bf16[2,256,512]{2,1,0:T(8,128)(2,1)S(1)} %broadcast_in_dim.23), channel_id=1, replica_groups=mesh['sp'=256,'tp'=2] {'tp'}, dimensions={0} | all-to-all | bytes 1048576 | tf_op jit(solution)/shard_map/all_to_all | solution.py:21
  110.9 1.0 copy.67
  (66 shorter events, 8.0 us)
Async XLA Ops:
  2.1 4.4 %copy-start.2 = (f32[2,1024]{1,0:T(2,128)S(1)}, f32[2,1024]{1,0:T(2,128)}, u32[]{:S(2)}) copy-start(f32[2,1024]{1,0:T(2,128)} %param.9) | copy-start | bytes 24580
  2.1 6.1 %all-to-all-start = ((bf16[2,512,512]{2,1,0:T(8,128)(2,1)}), bf16[2,512,512]{2,1,0:T(8,128)(2,1)S(1)}, u32[]{:S(2)}, u32[]{:S(2)}) async-start(bf16[2,512,512]{2,1,0:T(8,128)(2,1)} %broadcast_in_dim.16), calls=%async_computation | async-start | bytes 2097152 | tf_op jit(solution)/shard_map/all_to_all | solution.py:21
  8.5 1.2 %copy-start.5 = (bf16[2,256,1024]{2,1,0:T(8,128)(2,1)S(1)}, bf16[2,256,1024]{2,1,0:T(8,128)(2,1)}, u32[]{:S(2)}) copy-start(bf16[2,256,1024]{2,1,0:T(8,128)(2,1)} %param.10) | copy-start | bytes 3145732
  9.7 1.2 %copy-start.7 = (bf16[2,256,1024]{2,1,0:T(8,128)(2,1)S(1)}, bf16[2,256,1024]{2,1,0:T(8,128)(2,1)}, u32[]{:S(2)}) copy-start(bf16[2,256,1024]{2,1,0:T(8,128)(2,1)} %param.11) | copy-start | bytes 3145732
  11.0 11.1 %copy-start.3 = (f32[2,256]{1,0:T(2,128)S(1)}, f32[2,256]{1,0:T(2,128)}, u32[]{:S(2)}) copy-start(f32[2,256]{1,0:T(2,128)} %param.14) | copy-start | bytes 6148
  11.0 11.1 %copy-start.1 = (bf16[2,256,255]{1,0,2:T(2,128)(2,1)S(1)}, bf16[2,256,255]{1,0,2:T(2,128)(2,1)}, u32[]{:S(2)}) copy-start(bf16[2,256,255]{1,0,2:T(2,128)(2,1)} %param.12) | copy-start | bytes 783364
  11.5 11.0 %copy-start.4 = (f32[2,256]{1,0:T(2,128)S(1)}, f32[2,256]{1,0:T(2,128)}, u32[]{:S(2)}) copy-start(f32[2,256]{1,0:T(2,128)} %param.13) | copy-start | bytes 6148
  11.5 11.0 %copy-start = (bf16[512,512]{1,0:T(8,128)(2,1)S(1)}, bf16[512,512]{1,0:T(8,128)(2,1)}, u32[]{:S(2)}) copy-start(bf16[512,512]{1,0:T(8,128)(2,1)} %param.8) | copy-start | bytes 1572868
  11.5 11.6 %collective-permute-start.1 = (bf16[256,127]{0,1:T(8,128)(2,1)S(1)}, bf16[256,127]{0,1:T(8,128)(2,1)S(1)}, u32[]{:S(2)}, u32[]{:S(2)}) collective-permute-start(bf16[256,127]{0,1:T(8,128)(2,1)S(1)} %get-tuple-element.10), channel_id=1, source_target_pairs={{2,0},{4,2},{6,4},{8,6},{10,8},{12,10},{14,12},{16,14},{18,16},{20... | collective-permute-start | bytes 195080 | tf_op jit(solution)/shard_map/ppermute | solution.py:40
  20.2 10.4 %collective-permute-start = (bf16[256,127]{0,1:T(8,128)(2,1)S(1)}, bf16[256,127]{0,1:T(8,128)(2,1)S(1)}, u32[]{:S(2)}, u32[]{:S(2)}) collective-permute-start(bf16[256,127]{0,1:T(8,128)(2,1)S(1)} %get-tuple-element.9), channel_id=1, source_target_pairs={{0,2},{2,4},{4,6},{6,8},{8,10},{10,12},{12,14},{14,16},{16,18},{18... | collective-permute-start | bytes 195080 | tf_op jit(solution)/shard_map/ppermute | solution.py:38
  54.4 5.8 %copy-start.9 = (bf16[2,512,512]{2,1,0:T(8,128)(2,1)S(1)}, bf16[2,512,512]{2,1,0:T(8,128)(2,1)}, u32[]{:S(2)}) copy-start(bf16[2,512,512]{2,1,0:T(8,128)(2,1)} %param.15) | copy-start | bytes 3145732
  65.9 1.2 %copy-start.6 = (bf16[2,256,1024]{2,1,0:T(8,128)(2,1)S(1)}, bf16[2,256,1024]{2,1,0:T(8,128)(2,1)}, u32[]{:S(2)}) copy-start(bf16[2,256,1024]{2,1,0:T(8,128)(2,1)} %param.10) | copy-start | bytes 3145732
  67.1 1.2 %copy-start.8 = (bf16[2,256,1024]{2,1,0:T(8,128)(2,1)S(1)}, bf16[2,256,1024]{2,1,0:T(8,128)(2,1)}, u32[]{:S(2)}) copy-start(bf16[2,256,1024]{2,1,0:T(8,128)(2,1)} %param.11) | copy-start | bytes 3145732
  68.9 5.7 %collective-permute-start.3 = (bf16[256,127]{0,1:T(8,128)(2,1)S(1)}, bf16[256,127]{0,1:T(8,128)(2,1)S(1)}, u32[]{:S(2)}, u32[]{:S(2)}) collective-permute-start(bf16[256,127]{0,1:T(8,128)(2,1)S(1)} %get-tuple-element.8), channel_id=1, source_target_pairs={{2,0},{4,2},{6,4},{8,6},{10,8},{12,10},{14,12},{16,14},{18,16},{20... | collective-permute-start | bytes 195080 | tf_op jit(solution)/shard_map/ppermute | solution.py:40
  70.8 10.4 %collective-permute-start.2 = (bf16[256,127]{0,1:T(8,128)(2,1)S(1)}, bf16[256,127]{0,1:T(8,128)(2,1)S(1)}, u32[]{:S(2)}, u32[]{:S(2)}) collective-permute-start(bf16[256,127]{0,1:T(8,128)(2,1)S(1)} %get-tuple-element.7), channel_id=1, source_target_pairs={{0,2},{2,4},{4,6},{6,8},{8,10},{10,12},{12,14},{14,16},{16,18},{18... | collective-permute-start | bytes 195080 | tf_op jit(solution)/shard_map/ppermute | solution.py:38
  105.0 5.4 %copy-start.10 = (bf16[2,512,512]{2,1,0:T(8,128)(2,1)S(1)}, bf16[2,512,512]{2,1,0:T(8,128)(2,1)}, u32[]{:S(2)}) copy-start(bf16[2,512,512]{2,1,0:T(8,128)(2,1)} %param.15) | copy-start | bytes 3145732
where the time goes:
time: 113 us; the launch traced here: 112 us
  matrix products  43.1 us (38%)
  starting transfers between devices  20.2 us (18%)
  waiting for transfers between devices  15.9 us (14%)
  blocking collectives  15.7 us (14%)
  local copies, waits for them, and re-layouts  10.2 us (9%)
  other arithmetic  6.41 us (6%)
    conv_general_dilated x2, matrix products, filter_norm(): lax.conv_general_dilated(padded[None], taps[:, None, :], (1,), [(0, 0)],...  40.1 us
    all_to_all x3, blocking collectives, sent_to_all(): lax.all_to_all(jnp.broadcast_to(value[None], (count, *value.shape)), axis...  15.7 us
    ppermute x2, waiting for transfers between devices, with_halo(): lax.ppermute(tail, axis, [(i, (i + 1) % count) for i in range(ends)])  14.2 us
    ppermute x2, starting transfers between devices, with_halo(): lax.ppermute(head, axis, [((i + 1) % count, i) for i in range(ends)])  10.5 us
    ppermute x2, starting transfers between devices, with_halo(): lax.ppermute(tail, axis, [(i, (i + 1) % count) for i in range(ends)])  5.28 us
    all_to_all x1, starting transfers between devices, sent_to_all(): lax.all_to_all(jnp.broadcast_to(value[None], (count, *value.shape)), axis...  4.37 us
    unnamed x27, local copies, waits for them, and re-layouts  4.11 us
    reduce_sum x2, other arithmetic, filter_norm(): jnp.mean(centred * centred, axis=1, keepdims=True) + LN_EPS  3.18 us
  transfers between devices with their start and end apart: 5, of which 3 were waited for; matrix products, arithmetic and copies ran while one was open for 1% of the time, Pallas kernels for 0%

commit v1 on v0

v1 whole, which is shorter than its diff:
```python
import jax
import jax.numpy as jnp
import numpy as np
from jax import lax
from jax.sharding import PartitionSpec as P

GROUP_DIM = 128


RMS_EPS = 1e-06
LN_EPS = 1e-05

WINDOW = 512
KEPT = 256
FIRST = 128


def split_table(table):
    high = table.astype(jnp.bfloat16)
    low = (table - high.astype(np.float64)).astype(jnp.bfloat16)
    return high, low


def transform_tables(taps):
    bins = 2 * np.arange(WINDOW // 2) + 1
    reach = (taps - 1) // 2

    def angles(left, right):
        return np.pi * (np.outer(left, right) % (2 * WINDOW)) / WINDOW

    time = angles(np.arange(WINDOW), bins)
    forward = np.concatenate([np.cos(time), -np.sin(time)], 1)
    lag = angles(np.arange(taps) - reach, bins)
    tap_side = np.concatenate([np.cos(lag), np.sin(lag)], 1) * (2.0 / WINDOW)
    back = angles(bins, np.arange(FIRST, FIRST + KEPT))
    inverse = np.concatenate([np.cos(back), -np.sin(back)], 0)
    fh, fl = split_table(forward)
    th, tl = split_table(tap_side)
    ih, il = split_table(inverse)
    return (
        np.concatenate([fh, fl], 0),
        np.concatenate([th, tl], 0),
        np.concatenate([ih, ih, il], 0),
    )


def gathered(value, dim):
    return lax.all_gather(value, "tp", axis=dim, tiled=True)


def dot(a, b):
    return jnp.dot(a, b, preferred_element_type=jnp.float32)


def with_halo(cells, width):
    count = lax.axis_size("sp")
    ends = count - 1
    head = cells[:, :width]
    tail = cells[:, cells.shape[1] - width :]
    return jnp.concatenate(
        [
            lax.ppermute(tail, "sp", [(i, i + 1) for i in range(ends)]),
            cells,
            lax.ppermute(head, "sp", [(i + 1, i) for i in range(ends)]),
        ],
        axis=1,
    )


def make_gated(whole, gain, value_weight, gate_weight):
    widened = whole.astype(jnp.float32)
    inverse_rms = lax.rsqrt(jnp.mean(widened * widened, axis=0, keepdims=True) + RMS_EPS)
    normed = (widened * inverse_rms * gain[:, None]).astype(jnp.bfloat16)
    projected = dot(value_weight, normed).astype(jnp.bfloat16)
    gate_proj = dot(gate_weight, normed).astype(jnp.bfloat16)
    return (projected.astype(jnp.float32) * jax.nn.sigmoid(gate_proj.astype(jnp.float32))).astype(
        jnp.bfloat16
    )


def filter_norm(padded, tap_bins, tables, ggain, gshift):
    channels = padded.shape[0]
    half = WINDOW // 2
    tap_re, tap_im = tap_bins[:, :half], tap_bins[:, half:]
    kept = []
    for start in range(0, padded.shape[1] - KEPT, KEPT):
        piece = padded[:, start : start + WINDOW]
        freq = dot(jnp.concatenate([piece, piece], 1), tables[0])
        re, im = freq[:, :half], freq[:, half:]
        prod = jnp.concatenate([re * tap_re - im * tap_im, re * tap_im + im * tap_re], 1)
        high = prod.astype(jnp.bfloat16)
        low = (prod - high.astype(jnp.float32)).astype(jnp.bfloat16)
        kept.append(dot(jnp.concatenate([high, low, high], 1), tables[2]))
    filtered = jnp.concatenate(kept, 1)
    tokens_here = filtered.shape[1]
    grouped = filtered.reshape(channels // GROUP_DIM, GROUP_DIM, tokens_here)
    group_mean = jnp.mean(grouped, axis=1, keepdims=True)
    centred = grouped - group_mean
    scaled = centred * lax.rsqrt(jnp.mean(centred * centred, axis=1, keepdims=True) + LN_EPS)
    scaled = scaled.reshape(channels, tokens_here) * ggain[:, None] + gshift[:, None]
    return jax.nn.silu(scaled).astype(jnp.bfloat16)


def body(stream, norm_gain, w_value, w_gate, conv_taps, group_gain, group_shift, w_out):
    taps = conv_taps.shape[2]
    layers = w_value.shape[0]
    tables = transform_tables(taps)
    for layer_index in range(layers):
        part = stream.shape[0] // 2
        tokens = stream.shape[1]
        low_rows = lax.all_gather(stream[:part], "tp", axis=0)
        high_rows = lax.all_gather(stream[part:], "tp", axis=0)
        whole = jnp.stack([low_rows, high_rows], 1).reshape(-1, tokens)
        gated = make_gated(whole, norm_gain[layer_index], w_value[layer_index], w_gate[layer_index])
        padded = with_halo(gated, 128)
        both = jnp.concatenate([conv_taps[layer_index]] * 2, 1)
        tap_bins = dot(both, tables[1])
        activated = filter_norm(
            padded, tap_bins, tables, group_gain[layer_index], group_shift[layer_index]
        )
        branch = dot(w_out[layer_index], gathered(activated, 0))
        stream = (stream.astype(jnp.float32) + branch).astype(jnp.bfloat16)
    return stream


def solution(mesh):
    placed = (
        P("tp", "sp"),
        P(),
        P(None, "tp", None),
        P(None, "tp", None),
        P(None, "tp", None),
        P(None, "tp"),
        P(None, "tp"),
        P(None, "tp", None),
    )
    return jax.shard_map(body, mesh=mesh, in_specs=placed, out_specs=P("tp", "sp"), check_vma=False)
```

time: 113 us -> 79 us (0.70)
  matrix products: 43.1 us -> 9.66 us
  local copies, waits for them, and re-layouts: 10.2 us -> 15.5 us
  starting transfers between devices: 20.2 us -> 16.2 us
  waiting for transfers between devices: 15.9 us -> 12.5 us
    conv_general_dilated x2 -> x0, matrix products: 40.1 us -> none  [filter_norm(): lax.conv_general_dilated(padded[None], taps[:, None, :], (1,), [(0, 0)],...]
    all_gather x0 -> x6, blocking collectives: none -> 16.7 us  [the longest x2 7.48 us: gathered(): return lax.all_gather(value, 'tp', axis=dim, tiled=True)]
    all_to_all x3 -> x0, blocking collectives: 15.7 us -> none  [sent_to_all(): lax.all_to_all(jnp.broadcast_to(value[None], (count, *value.shape)), axis...]
    dot_general x6 -> x30, matrix products: 2.94 us -> 9.66 us  [dot(): return jnp.dot(a, b, preferred_element_type=jnp.float32)]
    all_to_all x1 -> x0, starting transfers between devices: 4.37 us -> none  [sent_to_all(): lax.all_to_all(jnp.broadcast_to(value[None], (count, *value.shape)), axis...]
    unnamed x27 -> x47, local copies, waits for them, and re-layouts: 4.11 us -> 6.97 us
    broadcast_in_dim x4 -> x0, local copies, waits for them, and re-layouts: 2.24 us -> none  [sent_to_all(): jnp.broadcast_to(value[None], (count, *value.shape))]
    all_to_all x1 -> x0, waiting for transfers between devices: 1.7 us -> none  [sent_to_all(): lax.all_to_all(jnp.broadcast_to(value[None], (count, *value.shape)), axis...]
  transfers between devices with their start and end apart: 5 -> 4, of which waited for: 3 -> 2; matrix products, arithmetic and copies ran while one was open for 1% -> 5% of each run, Pallas kernels for 0% -> 0%
where the time goes in v1:
time: 79 us; the launch traced here: 78.4 us
  blocking collectives  16.7 us (21%)
  starting transfers between devices  16.2 us (21%)
  local copies, waits for them, and re-layouts  15.5 us (20%)
  waiting for transfers between devices  12.5 us (16%)
  matrix products  9.66 us (12%)
  other arithmetic  7.15 us (9%)
    ppermute x2, waiting for transfers between devices, with_halo(): lax.ppermute(tail, 'sp', [(i, i + 1) for i in range(ends)])  12.5 us
    ppermute x2, starting transfers between devices, with_halo(): lax.ppermute(head, 'sp', [(i + 1, i) for i in range(ends)])  12.1 us
    dot_general x30, matrix products, dot(): return jnp.dot(a, b, preferred_element_type=jnp.float32)  9.66 us
    all_gather x2, blocking collectives, gathered(): return lax.all_gather(value, 'tp', axis=dim, tiled=True)  7.48 us
    unnamed x47, local copies, waits for them, and re-layouts  6.97 us
    all_gather x2, blocking collectives, body(): low_rows = lax.all_gather(stream[:part], 'tp', axis=0)  4.65 us
    all_gather x2, blocking collectives, body(): high_rows = lax.all_gather(stream[part:], 'tp', axis=0)  4.61 us
    ppermute x2, starting transfers between devices, with_halo(): lax.ppermute(tail, 'sp', [(i, i + 1) for i in range(ends)])  4.02 us
  transfers between devices with their start and end apart: 4, of which 2 were waited for; matrix products, arithmetic and copies ran while one was open for 5% of the time, Pallas kernels for 0%

profile of v1, /device:TPU:385, one launch (start us, length us, event | category | flops | bytes accessed | tf_op | source)
XLA Modules:
  0.0 78.4 jit_solution(3508970559193231017)
XLA Ops:
  0.0 1.1 %fusion.97 = (bf16[256,512]{1,0:T(8,128)(2,1)S(1)}, bf16[256,512]{1,0:T(8,128)(2,1)S(1)}) fusion(bf16[512,512]{1,0:T(8,128)(2,1)} %param.11), kind=kLoop, calls=%fused_computation.149 | loop fusion | bytes 1048576 | tf_op jit(solution)/shard_map/slice | solution.py:111
  1.1 2.5 %all-gather = bf16[512,512]{1,0:T(8,128)(2,1)S(1)} all-gather(bf16[256,512]{1,0:T(8,128)(2,1)S(1)} %get-tuple-element.21), channel_id=2, replica_groups=mesh['sp'=256,'tp'=2] {'tp'}, dimensions={0}, use_global_device_ids=true | all-gather | bytes 786432 | tf_op jit(solution)/shard_map/all_gather | solution.py:111
  3.6 2.3 %all-gather.1 = bf16[512,512]{1,0:T(8,128)(2,1)S(1)} all-gather(bf16[256,512]{1,0:T(8,128)(2,1)S(1)} %get-tuple-element.22), channel_id=3, replica_groups=mesh['sp'=256,'tp'=2] {'tp'}, dimensions={0}, use_global_device_ids=true | all-gather | bytes 786432 | tf_op jit(solution)/shard_map/all_gather | solution.py:112
  6.5 0.9 %copy-done.16 = bf16[2,256,1024]{2,1,0:T(8,128)(2,1)S(1)} copy-done((bf16[2,256,1024]{2,1,0:T(8,128)(2,1)S(1)}, bf16[2,256,1024]{2,1,0:T(8,128)(2,1)}, u32[]{:S(2)}) %copy-start.16) | copy-done | bytes 1048600
  9.2 8.6 %collective-permute-start.1 = (bf16[256,128]{0,1:T(8,128)(2,1)S(1)}, bf16[256,128]{0,1:T(8,128)(2,1)S(1)}, u32[]{:S(2)}, u32[]{:S(2)}) collective-permute-start(bf16[256,128]{0,1:T(8,128)(2,1)S(1)} %get-tuple-element.26), channel_id=1, source_target_pairs={{2,0},{4,2},{6,4},{8,6},{10,8},{12,10},{14,12},{16,14},{18,16},{20... | collective-permute-start | bytes 196616 | tf_op jit(solution)/shard_map/ppermute | solution.py:64
  17.8 1.9 %collective-permute-start = (bf16[256,128]{0,1:T(8,128)(2,1)S(1)}, bf16[256,128]{0,1:T(8,128)(2,1)S(1)}, u32[]{:S(2)}, u32[]{:S(2)}) collective-permute-start(bf16[256,128]{0,1:T(8,128)(2,1)S(1)} %get-tuple-element.25), channel_id=1, source_target_pairs={{0,2},{2,4},{4,6},{6,8},{8,10},{10,12},{12,14},{14,16},{16,18},{18... | collective-permute-start | bytes 196616 | tf_op jit(solution)/shard_map/ppermute | solution.py:62
  22.1 1.0 %copy.20 = bf16[512,512]{0,1:T(8,128)(2,1)} copy(bf16[512,512]{1,0:T(8,128)(2,1)S(1)} %copy-done.4) | data formatting | bytes 1048576 | tf_op args[0]
  23.5 4.8 %collective-permute-done = bf16[256,128]{0,1:T(8,128)(2,1)S(1)} collective-permute-done((bf16[256,128]{0,1:T(8,128)(2,1)S(1)}, bf16[256,128]{0,1:T(8,128)(2,1)S(1)}, u32[]{:S(2)}, u32[]{:S(2)}) %collective-permute-start) | collective-permute-done | bytes 65568 | tf_op jit(solution)/shard_map/ppermute | solution.py:62
  29.4 0.8 %copy-done = bf16[512,256]{1,0:T(8,128)(2,1)S(1)} copy-done((bf16[512,256]{1,0:T(8,128)(2,1)S(1)}, bf16[512,256]{1,0:T(8,128)(2,1)}, u32[]{:S(2)}) %copy-start) | copy-done | bytes 262168
  32.3 0.8 %pad_maximum_fusion.4 = f32[256,512]{0,1:T(8,128)} fusion(f32[256,256]{0,1:T(8,128)S(1)} %convolution_add_fusion.10, f32[256,256]{0,1:T(8,128)S(1)} %convolution_add_fusion.12), kind=kLoop, calls=%fused_computation.66 | loop fusion | flops 131072 | bytes 1048576 | tf_op jit(solution)/shard_map/concatenate | solution.py:94
  33.1 1.3 %reshape.242 = f32[2,128,512]{1,0,2:T(2,128)S(1)} reshape(f32[256,512]{0,1:T(8,128)} %pad_maximum_fusion.4) | data formatting | bytes 1048576 | tf_op jit(solution)/shard_map/reshape | solution.py:96
  35.1 1.6 %multiply_reduce_fusion.1 = f32[2,512]{0,1:T(8,128)S(1)} fusion(f32[2,128,512]{1,0,2:T(2,128)S(1)} %reshape.242, f32[2,512]{0,1:T(8,128)S(1)} %broadcast_multiply_fusion.1), kind=kLoop, calls=%fused_computation.85 | loop fusion | flops 392192 | bytes 532480 | tf_op jit(solution)/shard_map/reduce_sum | solution.py:99
  38.2 3.7 %all_gather.34 = bf16[512,512]{0,1:T(8,128)(2,1)S(1)} all-gather(bf16[256,512]{0,1:T(8,128)(2,1)S(1)} %multiply_convert_fusion.1), channel_id=1, replica_groups=mesh['sp'=256,'tp'=2] {'tp'}, dimensions={0}, use_global_device_ids=true | all-gather | bytes 786432 | tf_op jit(solution)/shard_map/all_gather | solution.py:48
  42.4 0.7 copy-done.9
  43.2 2.2 %all-gather.2 = bf16[512,512]{0,1:T(8,128)(2,1)S(1)} all-gather(bf16[256,512]{0,1:T(8,128)(2,1)S(1)} %get-tuple-element.17), channel_id=4, replica_groups=mesh['sp'=256,'tp'=2] {'tp'}, dimensions={0}, use_global_device_ids=true | all-gather | bytes 786432 | tf_op jit(solution)/shard_map/all_gather | solution.py:111
  45.6 2.3 %all-gather.3 = bf16[512,512]{0,1:T(8,128)(2,1)} all-gather(bf16[256,512]{0,1:T(8,128)(2,1)S(1)} %get-tuple-element.18), channel_id=5, replica_groups=mesh['sp'=256,'tp'=2] {'tp'}, dimensions={0}, use_global_device_ids=true | all-gather | bytes 786432 | tf_op jit(solution)/shard_map/all_gather | solution.py:112
  47.9 1.3 %copy.35 = bf16[512,512]{1,0:T(8,128)(2,1)S(1)} copy(bf16[512,512]{0,1:T(8,128)(2,1)} %all-gather.3) | data formatting | bytes 1048576 | tf_op jit(solution)/shard_map/stack | solution.py:113
  49.7 0.9 %copy-done.17 = bf16[2,256,1024]{2,1,0:T(8,128)(2,1)S(1)} copy-done((bf16[2,256,1024]{2,1,0:T(8,128)(2,1)S(1)}, bf16[2,256,1024]{2,1,0:T(8,128)(2,1)}, u32[]{:S(2)}) %copy-start.17) | copy-done | bytes 1048600
  52.4 3.5 %collective-permute-start.3 = (bf16[256,128]{0,1:T(8,128)(2,1)S(1)}, bf16[256,128]{0,1:T(8,128)(2,1)S(1)}, u32[]{:S(2)}, u32[]{:S(2)}) collective-permute-start(bf16[256,128]{0,1:T(8,128)(2,1)S(1)} %get-tuple-element.24), channel_id=1, source_target_pairs={{2,0},{4,2},{6,4},{8,6},{10,8},{12,10},{14,12},{16,14},{18,16},{20... | collective-permute-start | bytes 196616 | tf_op jit(solution)/shard_map/ppermute | solution.py:64
  56.2 2.1 %collective-permute-start.2 = (bf16[256,128]{0,1:T(8,128)(2,1)S(1)}, bf16[256,128]{0,1:T(8,128)(2,1)S(1)}, u32[]{:S(2)}, u32[]{:S(2)}) collective-permute-start(bf16[256,128]{0,1:T(8,128)(2,1)S(1)} %get-tuple-element.23), channel_id=1, source_target_pairs={{0,2},{2,4},{4,6},{6,8},{8,10},{10,12},{12,14},{14,16},{16,18},{18... | collective-permute-start | bytes 196616 | tf_op jit(solution)/shard_map/ppermute | solution.py:62
  59.0 7.7 %collective-permute-done.2 = bf16[256,128]{0,1:T(8,128)(2,1)S(1)} collective-permute-done((bf16[256,128]{0,1:T(8,128)(2,1)S(1)}, bf16[256,128]{0,1:T(8,128)(2,1)S(1)}, u32[]{:S(2)}, u32[]{:S(2)}) %collective-permute-start.2) | collective-permute-done | bytes 65568 | tf_op jit(solution)/shard_map/ppermute | solution.py:62
  70.1 1.6 %multiply_reduce_fusion = f32[2,512]{0,1:T(8,128)S(1)} fusion(f32[2,128,512]{1,0,2:T(2,128)S(1)} %reshape.243, f32[2,512]{0,1:T(8,128)S(1)} %broadcast_multiply_fusion), kind=kLoop, calls=%fused_computation.78 | loop fusion | flops 392192 | bytes 532480 | tf_op jit(solution)/shard_map/reduce_sum | solution.py:99
  73.1 3.7 %all_gather.39 = bf16[512,512]{0,1:T(8,128)(2,1)S(1)} all-gather(bf16[256,512]{0,1:T(8,128)(2,1)S(1)} %multiply_convert_fusion), channel_id=1, replica_groups=mesh['sp'=256,'tp'=2] {'tp'}, dimensions={0}, use_global_device_ids=true | all-gather | bytes 786432 | tf_op jit(solution)/shard_map/all_gather | solution.py:48
  77.3 1.0 %copy.29 = bf16[512,512]{1,0:T(8,128)(2,1)} copy(bf16[512,512]{0,1:T(8,128)(2,1)S(1)} %fusion.9) | data formatting | bytes 1048576 | tf_op jit(solution)/shard_map/convert_element_type | solution.py:122
  (106 shorter events, 19.3 us)
Async XLA Ops:
  3.6 2.6 %copy-start.12 = (f32[2,1024]{1,0:T(2,128)S(1)}, f32[2,1024]{1,0:T(2,128)}, u32[]{:S(2)}) copy-start(f32[2,1024]{1,0:T(2,128)} %param.12) | copy-start | bytes 24580
  6.2 1.2 %copy-start.16 = (bf16[2,256,1024]{2,1,0:T(8,128)(2,1)S(1)}, bf16[2,256,1024]{2,1,0:T(8,128)(2,1)}, u32[]{:S(2)}) copy-start(bf16[2,256,1024]{2,1,0:T(8,128)(2,1)} %param.13) | copy-start | bytes 3145732
  7.4 1.2 %copy-start.18 = (bf16[2,256,1024]{2,1,0:T(8,128)(2,1)S(1)}, bf16[2,256,1024]{2,1,0:T(8,128)(2,1)}, u32[]{:S(2)}) copy-start(bf16[2,256,1024]{2,1,0:T(8,128)(2,1)} %param.14) | copy-start | bytes 3145732
  8.7 11.1 %copy-start.8 = (bf16[2,256,255]{1,0,2:T(2,128)(2,1)S(1)}, bf16[2,256,255]{1,0,2:T(2,128)(2,1)}, u32[]{:S(2)}) copy-start(bf16[2,256,255]{1,0,2:T(2,128)(2,1)} %param.15) | copy-start | bytes 783364
  9.2 11.2 %copy-start.14 = (f32[2,256]{1,0:T(2,128)S(1)}, f32[2,256]{1,0:T(2,128)}, u32[]{:S(2)}) copy-start(f32[2,256]{1,0:T(2,128)} %param.16) | copy-start | bytes 6148
  9.2 11.3 %copy-start.5 = (bf16[255,512]{1,0:T(8,128)(2,1)S(1)}, bf16[255,512]{1,0:T(8,128)(2,1)}, u32[]{:S(2)}) copy-start(bf16[255,512]{1,0:T(8,128)(2,1)} %constant.32) | copy-start | bytes 783364
  9.2 13.9 %collective-permute-start.1 = (bf16[256,128]{0,1:T(8,128)(2,1)S(1)}, bf16[256,128]{0,1:T(8,128)(2,1)S(1)}, u32[]{:S(2)}, u32[]{:S(2)}) collective-permute-start(bf16[256,128]{0,1:T(8,128)(2,1)S(1)} %get-tuple-element.26), channel_id=1, source_target_pairs={{2,0},{4,2},{6,4},{8,6},{10,8},{12,10},{14,12},{16,14},{18,16},{20... | collective-permute-start | bytes 196616 | tf_op jit(solution)/shard_map/ppermute | solution.py:64
  17.8 10.4 %collective-permute-start = (bf16[256,128]{0,1:T(8,128)(2,1)S(1)}, bf16[256,128]{0,1:T(8,128)(2,1)S(1)}, u32[]{:S(2)}, u32[]{:S(2)}) collective-permute-start(bf16[256,128]{0,1:T(8,128)(2,1)S(1)} %get-tuple-element.25), channel_id=1, source_target_pairs={{0,2},{2,4},{4,6},{6,8},{8,10},{10,12},{12,14},{14,16},{16,18},{18... | collective-permute-start | bytes 196616 | tf_op jit(solution)/shard_map/ppermute | solution.py:62
  20.3 1.0 %copy-start.6 = (bf16[255,512]{1,0:T(8,128)(2,1)S(1)}, bf16[255,512]{1,0:T(8,128)(2,1)}, u32[]{:S(2)}) copy-start(bf16[255,512]{1,0:T(8,128)(2,1)} %constant.33) | copy-start | bytes 783364
  20.8 1.4 %copy-start.4 = (bf16[512,512]{1,0:T(8,128)(2,1)S(1)}, bf16[512,512]{1,0:T(8,128)(2,1)}, u32[]{:S(2)}) copy-start(bf16[512,512]{1,0:T(8,128)(2,1)} %param.11) | copy-start | bytes 1572868
  21.3 1.9 %copy-start.1 = (bf16[512,512]{1,0:T(8,128)(2,1)S(1)}, bf16[512,512]{1,0:T(8,128)(2,1)}, u32[]{:S(2)}) copy-start(bf16[512,512]{1,0:T(8,128)(2,1)} %constant.31) | copy-start | bytes 1572868
  23.1 5.5 %copy-start.2 = (bf16[512,512]{1,0:T(8,128)(2,1)S(1)}, bf16[512,512]{1,0:T(8,128)(2,1)}, u32[]{:S(2)}) copy-start(bf16[512,512]{1,0:T(8,128)(2,1)} %constant.30) | copy-start | bytes 1572868
  29.3 1.0 %copy-start = (bf16[512,256]{1,0:T(8,128)(2,1)S(1)}, bf16[512,256]{1,0:T(8,128)(2,1)}, u32[]{:S(2)}) copy-start(bf16[512,256]{1,0:T(8,128)(2,1)} %constant.34) | copy-start | bytes 786436
  30.8 1.0 %copy-start.3 = (bf16[512,256]{1,0:T(8,128)(2,1)S(1)}, bf16[512,256]{1,0:T(8,128)(2,1)}, u32[]{:S(2)}) copy-start(bf16[512,256]{1,0:T(8,128)(2,1)} %constant.36) | copy-start | bytes 786436
  36.7 1.3 %copy-start.13 = (f32[1,256]{1,0:T(1,128)S(1)}, f32[1,256]{1,0:T(1,128)}, u32[]{:S(2)}) copy-start(f32[1,256]{1,0:T(1,128)} %get-tuple-element.32) | copy-start | bytes 3076
  37.9 3.9 %copy-start.11 = (bf16[512,512]{0,1:T(8,128)(2,1)S(1)}, bf16[512,512]{0,1:T(8,128)(2,1)}, u32[]{:S(2)}) copy-start(bf16[512,512]{0,1:T(8,128)(2,1)} %copy.20) | copy-start | bytes 1572868
  38.0 3.9 %copy-start.20 = (bf16[2,512,512]{2,1,0:T(8,128)(2,1)S(1)}, bf16[2,512,512]{2,1,0:T(8,128)(2,1)}, u32[]{:S(2)}) copy-start(bf16[2,512,512]{2,1,0:T(8,128)(2,1)} %param.18) | copy-start | bytes 3145732
  49.4 1.2 %copy-start.17 = (bf16[2,256,1024]{2,1,0:T(8,128)(2,1)S(1)}, bf16[2,256,1024]{2,1,0:T(8,128)(2,1)}, u32[]{:S(2)}) copy-start(bf16[2,256,1024]{2,1,0:T(8,128)(2,1)} %param.13) | copy-start | bytes 3145732
  50.7 1.2 %copy-start.19 = (bf16[2,256,1024]{2,1,0:T(8,128)(2,1)S(1)}, bf16[2,256,1024]{2,1,0:T(8,128)(2,1)}, u32[]{:S(2)}) copy-start(bf16[2,256,1024]{2,1,0:T(8,128)(2,1)} %param.14) | copy-start | bytes 3145732
  51.9 4.1 %copy-start.7 = (bf16[255,512]{1,0:T(8,128)(2,1)S(1)}, bf16[255,512]{1,0:T(8,128)(2,1)}, u32[]{:S(2)}) copy-start(bf16[255,512]{1,0:T(8,128)(2,1)} %constant.33) | copy-start | bytes 783364
  52.4 5.9 %collective-permute-start.3 = (bf16[256,128]{0,1:T(8,128)(2,1)S(1)}, bf16[256,128]{0,1:T(8,128)(2,1)S(1)}, u32[]{:S(2)}, u32[]{:S(2)}) collective-permute-start(bf16[256,128]{0,1:T(8,128)(2,1)S(1)} %get-tuple-element.24), channel_id=1, source_target_pairs={{2,0},{4,2},{6,4},{8,6},{10,8},{12,10},{14,12},{16,14},{18,16},{20... | collective-permute-start | bytes 196616 | tf_op jit(solution)/shard_map/ppermute | solution.py:64
  56.2 10.4 %collective-permute-start.2 = (bf16[256,128]{0,1:T(8,128)(2,1)S(1)}, bf16[256,128]{0,1:T(8,128)(2,1)S(1)}, u32[]{:S(2)}, u32[]{:S(2)}) collective-permute-start(bf16[256,128]{0,1:T(8,128)(2,1)S(1)} %get-tuple-element.23), channel_id=1, source_target_pairs={{0,2},{2,4},{4,6},{6,8},{8,10},{10,12},{12,14},{14,16},{16,18},{18... | collective-permute-start | bytes 196616 | tf_op jit(solution)/shard_map/ppermute | solution.py:62
  72.9 4.0 %copy-start.10 = (bf16[512,512]{0,1:T(8,128)(2,1)S(1)}, bf16[512,512]{0,1:T(8,128)(2,1)}, u32[]{:S(2)}) copy-start(bf16[512,512]{0,1:T(8,128)(2,1)} %copy-done.9) | copy-start | bytes 1572868
  72.9 3.9 %copy-start.21 = (bf16[2,512,512]{2,1,0:T(8,128)(2,1)S(1)}, bf16[2,512,512]{2,1,0:T(8,128)(2,1)}, u32[]{:S(2)}) copy-start(bf16[2,512,512]{2,1,0:T(8,128)(2,1)} %param.18) | copy-start | bytes 3145732
  (2 other events, 1.6 us)

commit v2 on v1

v2 whole, which is shorter than its diff:
```python
import functools

import jax
import jax.numpy as jnp
import numpy as np
from jax import lax
from jax.experimental import pallas as pl
from jax.experimental.pallas import tpu as pltpu
from jax.sharding import PartitionSpec as P


RMS_EPS = 1e-06
LN_EPS = 1e-05

WINDOW = 512
KEPT = 256
FIRST = 128
BINS = WINDOW // 2
TAP_ROW = 1536
GAIN_ROW = 1664
PACK_ROWS = 1680
HALF = 256


def transform_tables(taps):
    bins = 2 * np.arange(BINS) + 1
    reach = (taps - 1) // 2

    def angles(left, right):
        return np.pi * (np.outer(left, right) % (2 * WINDOW)) / WINDOW

    time = angles(np.arange(WINDOW), bins)
    lag = angles(np.arange(taps) - reach, bins)
    back = angles(bins, np.arange(FIRST, FIRST + KEPT))
    tap_side = np.concatenate([np.cos(lag), np.sin(lag)], 1) * (2.0 / WINDOW)
    tap_side = np.pad(tap_side, ((0, 256 - taps), (0, 0)))
    forward = np.concatenate([np.cos(time), -np.sin(time)], 1)
    inverse = np.concatenate([np.cos(back), -np.sin(back)], 0)

    def terms(table):
        high = table.astype(jnp.bfloat16)
        return high, (table - high.astype(np.float64)).astype(jnp.bfloat16)

    return np.concatenate(
        [*terms(tap_side), *terms(forward), np.concatenate(terms(inverse), 1)], 0
    )


def dot(a, b):
    return jnp.dot(a, b, preferred_element_type=jnp.float32)


def column(row):
    return jnp.transpose(jnp.broadcast_to(row, (128, 128)))


def wide(col):
    return jnp.concatenate([col, col], 1)


def sigmoid(value):
    return 0.5 * jnp.tanh(0.5 * value) + 0.5


def layers_kernel(
    place, own, near, far, halo, gain, pack, pack2, tables, keep, send,
    xw, normed, gated, act, x1, gated2, act2, bins, gains, gcols, table, sems,
):
    me = place[0]
    other = 1 - me
    packs = (pack, pack2)

    copies = [
        pltpu.make_async_copy(
            tables.at[pl.ds(start, size)], table.at[pl.ds(start, size)], sems.at[i]
        )
        for i, (start, size) in enumerate(((0, 512), (512, 1024), (1536, 512)))
    ]
    for copy in copies:
        copy.start()

    def lanes(block, size=HALF):
        return pl.ds(pl.multiple_of(block * size, size), size)

    first = other
    for part in range(2):
        xw[:512, lanes(first + part)] = own[:, part * HALF : (part + 1) * HALF]
    xw[512:, lanes(first + me)] = near[other]
    xw[512:, lanes(first + other)] = far[other]
    xw[512:, lanes(2 * me)] = halo[:512]
    xw[:512, lanes(2 * me)] = halo[512:]

    for layer in range(2):
        for half, block in enumerate((me, other)):
            for j in range(4):
                row = gain[layer : layer + 1, lanes(4 * block + j, 128)]
                start = half * 512 + j * 128
                gains[layer, start : start + 128] = column(row)
        for chunk, source in enumerate(packs):
            terms = source[GAIN_ROW : GAIN_ROW + 16, :256].astype(jnp.float32)
            for g in range(2):
                for kind in range(2):
                    t = terms[:, g * 128 : (g + 1) * 128]
                    i = 6 * layer + 3 * kind
                    row = t[i : i + 1] + t[i + 1 : i + 2] + t[i + 2 : i + 3]
                    start = chunk * 256 + g * 128
                    gcols[layer, kind, start : start + 128] = column(row)

    def norm(source, tile, layer, slot):
        cols = slice(tile * HALF, (tile + 1) * HALF)
        total = jnp.zeros((8, HALF), jnp.float32)
        for r in range(0, 1024, 128):
            piece = source[r : r + 128, cols].astype(jnp.float32)
            square = piece * piece
            for s in range(0, 128, 8):
                total += square[s : s + 8]
        mean = jnp.sum(total, axis=0, keepdims=True) * (1.0 / 1024.0)
        inverse = lax.rsqrt(mean + RMS_EPS)
        for j in range(8):
            r = slice(j * 128, (j + 1) * 128)
            piece = source[r, cols].astype(jnp.float32)
            normed[slot, r, :] = (piece * inverse * wide(gains[layer, r])).astype(jnp.bfloat16)

    def project(slot, layer, target, tile):
        cols = slice(tile * HALF, (tile + 1) * HALF)
        for chunk, source in enumerate(packs):
            def product(start):
                r = slice(start + layer * 256, start + (layer + 1) * 256)
                total = dot(source[r, lanes(me, 512)], normed[slot, :512])
                return total + dot(source[r, lanes(other, 512)], normed[slot, 512:])

            projected = product(0).astype(jnp.bfloat16).astype(jnp.float32)
            gate_proj = product(512).astype(jnp.bfloat16).astype(jnp.float32)
            target[chunk * 256 : (chunk + 1) * 256, cols] = (
                projected * sigmoid(gate_proj)
            ).astype(jnp.bfloat16)

    def make_bins(layer):
        for chunk, source in enumerate(packs):
            for part in range(2):
                lane = (2 * layer + part) * 256
                taps = source[TAP_ROW : TAP_ROW + 128, lane : lane + 256]
                start = chunk * 256 + part * 128
                bins[layer, start : start + 128] = dot(taps, table[:256]) + dot(
                    taps, table[256:512]
                )

    def filter_norm(source, start, layer, target):
        for chunk in range(2):
            r = slice(chunk * 256, (chunk + 1) * 256)
            piece = source[r, start : start + WINDOW]
            freq = dot(piece, table[512:1024]) + dot(piece, table[1024:1536])
            re, im = freq[:, :BINS], freq[:, BINS:]
            tap_re, tap_im = bins[layer, r, :BINS], bins[layer, r, BINS:]
            prod = jnp.concatenate(
                [re * tap_re - im * tap_im, re * tap_im + im * tap_re], 1
            )
            high = prod.astype(jnp.bfloat16)
            low = (prod - high.astype(jnp.float32)).astype(jnp.bfloat16)
            ih, il = table[1536:2048, :KEPT], table[1536:2048, KEPT:]
            filtered = dot(high, ih) + dot(low, ih) + dot(high, il)
            for g in range(2):
                v = filtered[g * 128 : (g + 1) * 128]
                c = slice(chunk * 256 + g * 128, chunk * 256 + (g + 1) * 128)
                centred = v - jnp.mean(v, axis=0, keepdims=True)
                var = jnp.mean(centred * centred, axis=0, keepdims=True)
                scaled = centred * lax.rsqrt(var + LN_EPS)
                scaled = scaled * wide(gcols[layer, 0, c]) + wide(gcols[layer, 1, c])
                target[c, :] = (scaled * sigmoid(scaled)).astype(jnp.bfloat16)

    def branch(source, layer, activated):
        r = slice(1024, 1536)
        total = dot(source[r, lanes(2 * layer + me)], activated[:256])
        return total + dot(source[r, lanes(2 * layer + other)], activated[256:])

    lane = lax.broadcasted_iota(jnp.int32, (8, KEPT), 1)
    outside = (
        (lane < FIRST) & (place[1] == 1),
        (lane >= KEPT - FIRST) & (place[2] == 1),
    )

    def finish_first(b):
        cols = slice(FIRST + b * KEPT, FIRST + (b + 1) * KEPT)
        for half, source in enumerate(packs):
            r = slice(half * 512, (half + 1) * 512)
            total = xw[r, cols].astype(jnp.float32) + branch(source, 0, act[b])
            drop = jnp.broadcast_to(outside[b][:1], total.shape)
            total = jnp.where(drop, 0.0, total)
            x1[r, b * KEPT : (b + 1) * KEPT] = total.astype(jnp.bfloat16)

    norm(xw, 0, 0, 0)
    norm(xw, 1, 0, 1)
    copies[0].wait()
    make_bins(0)
    project(0, 0, gated, 0)
    norm(xw, 2, 0, 2)
    project(1, 0, gated, 1)
    copies[1].wait()
    copies[2].wait()
    filter_norm(gated, 0, 0, act.at[0])
    project(2, 0, gated, 2)
    finish_first(0)
    filter_norm(gated, KEPT, 0, act.at[1])
    norm(x1, 0, 1, 3)
    finish_first(1)
    make_bins(1)
    project(3, 1, gated2, 0)
    norm(x1, 1, 1, 4)
    project(4, 1, gated2, 1)
    filter_norm(gated2, 0, 1, act2)
    cols = slice(FIRST, FIRST + KEPT)
    for half, (source, out) in enumerate(((pack, keep), (pack2, send))):
        before = x1[half * 512 : (half + 1) * 512, cols].astype(jnp.float32)
        out[...] = (before + branch(source, 1, act2)).astype(jnp.bfloat16)


def run_layers(place, arrays):
    vmem = pl.BlockSpec(memory_space=pltpu.VMEM)
    out = jax.ShapeDtypeStruct((512, KEPT), jnp.bfloat16)
    return pl.pallas_call(
        layers_kernel,
        out_shape=[out, out],
        in_specs=[pl.BlockSpec(memory_space=pltpu.SMEM)]
        + [vmem] * (len(arrays) - 1)
        + [pl.BlockSpec(memory_space=pltpu.HBM)],
        out_specs=[vmem, vmem],
        scratch_shapes=[
            pltpu.VMEM((1024, 768), jnp.bfloat16),
            pltpu.VMEM((5, 1024, HALF), jnp.bfloat16),
            pltpu.VMEM((512, 768), jnp.bfloat16),
            pltpu.VMEM((2, 512, KEPT), jnp.bfloat16),
            pltpu.VMEM((1024, 512), jnp.bfloat16),
            pltpu.VMEM((512, 512), jnp.bfloat16),
            pltpu.VMEM((512, KEPT), jnp.bfloat16),
            pltpu.VMEM((2, 512, WINDOW), jnp.float32),
            pltpu.VMEM((2, 1024, 128), jnp.float32),
            pltpu.VMEM((2, 2, 512, 128), jnp.float32),
            pltpu.VMEM((2048, 512), jnp.bfloat16),
            pltpu.SemaphoreType.DMA((3,)),
        ],
        compiler_params=pltpu.CompilerParams(vmem_limit_bytes=28 << 20),
        cost_estimate=pl.CostEstimate(
            flops=7 * 10**9, bytes_accessed=10**7, transcendentals=2 * 10**6
        ),
    )(place, *arrays)


def pack_kernel(after, wv, wg, wo, taps0, taps1, ggain, gshift, out, sems):
    copies = []
    for layer in range(2):
        for start, source in ((0, wv), (512, wg)):
            copies.append((source.at[layer], out.at[pl.ds(start + layer * 256, 256)]))
        copies.append((wo.at[layer], out.at[pl.ds(1024, 512), pl.ds(512 * layer, 512)]))
    copies = [
        pltpu.make_async_copy(source, target, sems.at[i])
        for i, (source, target) in enumerate(copies)
    ]
    for copy in copies:
        copy.start()
    for layer, taps in enumerate((taps0, taps1)):
        for chunk in range(2):
            lane = (2 * layer + chunk) * 256
            piece = jnp.pad(taps[chunk * 128 : (chunk + 1) * 128], ((0, 0), (0, 1)))
            out[TAP_ROW : TAP_ROW + 128, lane : lane + 256] = piece
    rows = []
    for layer in range(2):
        for source in (ggain, gshift):
            rest = source[layer : layer + 1]
            for _ in range(3):
                term = rest.astype(jnp.bfloat16).astype(jnp.float32)
                rows.append(term)
                rest = rest - term
    rows.append(jnp.zeros((4, 256), jnp.float32))
    rows = jnp.concatenate(rows, 0).astype(jnp.bfloat16)
    out[GAIN_ROW:PACK_ROWS, :] = jnp.concatenate([rows, rows, rows, rows], 1)
    for copy in copies:
        copy.wait()


def run_pack(after, wv, wg, wo, taps, ggain, gshift):
    vmem = pl.BlockSpec(memory_space=pltpu.VMEM)
    anywhere = pl.BlockSpec(memory_space=pltpu.HBM)
    after_spec = pl.BlockSpec(memory_space=pl.ANY)
    return pl.pallas_call(
        pack_kernel,
        out_shape=jax.ShapeDtypeStruct((PACK_ROWS, 1024), jnp.bfloat16),
        in_specs=[after_spec] + [anywhere] * 3 + [vmem] * 4,
        out_specs=vmem,
        scratch_shapes=[pltpu.SemaphoreType.DMA((6,))],
        compiler_params=pltpu.CompilerParams(vmem_limit_bytes=8 << 20),
        cost_estimate=pl.CostEstimate(
            flops=2 * 10**9, bytes_accessed=7 * 10**6, transcendentals=0
        ),
    )(after, wv, wg, wo, taps[0], taps[1], ggain, gshift)


def body(blocks, stream, norm_gain, w_value, w_gate, conv_taps, group_gain, group_shift, w_out):
    taps = conv_taps.shape[2]
    me = lax.axis_index("tp")
    block = lax.axis_index("sp")
    both = ("sp", "tp")
    partner = [(i, i ^ 1) for i in range(2 * blocks)]
    outward = [(2 * s + 1, 2 * s + 2) for s in range(blocks - 1)]
    outward += [(2 * s + 2, 2 * s + 1) for s in range(blocks - 1)]

    outer = lax.dynamic_slice_in_dim(stream, HALF * me, HALF, 1)
    inner = lax.dynamic_slice_in_dim(stream, HALF * (1 - me), HALF, 1)
    near = lax.all_gather(inner, "tp", axis=0)
    mine = jnp.concatenate([outer, lax.dynamic_index_in_dim(near, 1 - me, 0, False)], 0)
    tables = jnp.asarray(transform_tables(taps))
    mine, conv_taps = lax.optimization_barrier((mine, conv_taps))
    halo = lax.ppermute(mine, both, outward)
    pack = run_pack(mine, w_value, w_gate, w_out, conv_taps, group_gain, group_shift)
    pack2 = lax.ppermute(pack, both, partner)
    far = lax.all_gather(outer, "tp", axis=0)

    place = jnp.stack(
        [me, (me == 0) & (block == 0), (me == 1) & (block == blocks - 1)]
    ).astype(jnp.int32)
    keep, send = run_layers(
        place,
        [stream, near, far, halo, norm_gain, pack, pack2, tables],
    )
    swapped = lax.all_gather(send, "tp", axis=0)
    return jnp.concatenate(
        [jnp.where(me == 0, keep, swapped[0]), jnp.where(me == 0, swapped[1], keep)], 1
    )


def solution(mesh):
    placed = (
        P("tp", "sp"),
        P(),
        P(None, "tp", None),
        P(None, "tp", None),
        P(None, "tp", None),
        P(None, "tp"),
        P(None, "tp"),
        P(None, "tp", None),
    )
    return jax.shard_map(
        functools.partial(body, mesh.shape["sp"]),
        mesh=mesh, in_specs=placed, out_specs=P("tp", "sp"), check_vma=False,
    )
```

time: 79 us -> 45.9 us (0.58)
  the two profiles are of different devices: /device:TPU:385 before, /device:TPU:1 now
where the time goes in v2:
time: 45.9 us; the launch traced here: 45.6 us
  Pallas kernels  15.5 us (34%)
  blocking collectives  15.1 us (33%)
  local copies, waits for them, and re-layouts  5.46 us (12%)
  waiting for transfers between devices  4.23 us (9%)
  starting transfers between devices  4.2 us (9%)
  other arithmetic  0.99 us (2%)
    pallas_call x1, Pallas kernels, run_layers(): pl.pallas_call(layers_kernel, out_shape=[out, out], in_specs=[pl.BlockSpe...  13.4 us
    all_gather x1, blocking collectives, body(): near = lax.all_gather(inner, 'tp', axis=0)  8.62 us
    all_gather x1, blocking collectives, body(): far = lax.all_gather(outer, 'tp', axis=0)  4.25 us
    ppermute x1, waiting for transfers between devices, body(): halo = lax.ppermute(mine, both, outward)  4.23 us
    unnamed x18, local copies, waits for them, and re-layouts  4.05 us
    ppermute x1, starting transfers between devices, body(): pack2 = lax.ppermute(pack, both, partner)  2.28 us
    all_gather x1, blocking collectives, body(): swapped = lax.all_gather(send, 'tp', axis=0)  2.18 us
    pallas_call x1, Pallas kernels, run_pack(): pl.pallas_call(pack_kernel, out_shape=jax.ShapeDtypeStruct((PACK_ROWS, 10...  2.14 us
  transfers between devices with their start and end apart: 2, of which 1 were waited for; matrix products, arithmetic and copies ran while one was open for 0% of the time, Pallas kernels for 0%

profile of v2, /device:TPU:1, one launch (start us, length us, event | category | flops | bytes accessed | tf_op | source)
XLA Modules:
  0.0 45.6 jit_solution(4698402151506627055)
XLA Ops:
  0.0 0.0 copy-start.1
  0.0 1.2 %constant_dynamic-slice_fusion = (bf16[512,256]{1,0:T(8,128)(2,1)S(1)}, bf16[512,256]{1,0:T(8,128)(2,1)S(1)}) fusion(bf16[512,512]{1,0:T(8,128)(2,1)} %own.1, s32[]{:T(128)S(6)} %select_n.24, s32[]{:T(128)S(6)} %select_n.23), kind=kLoop, calls=%fused_computation.7 | loop fusion | bytes 1048584 | tf_op jit(solution)/shard_map/dynamic_slice | solution.py:306
  1.2 8.6 %all-gather = bf16[1024,256]{1,0:T(8,128)(2,1)S(1)} all-gather(bf16[512,256]{1,0:T(8,128)(2,1)S(1)} %get-tuple-element.16), channel_id=2, replica_groups=mesh['sp'=256,'tp'=2] {'tp'}, dimensions={0}, use_global_device_ids=true | all-gather | bytes 786432 | tf_op jit(solution)/shard_map/all_gather | solution.py:308
  9.9 0.0 copy-done.8
  9.9 0.2 copy.10
  10.1 0.0 copy-done.6
  10.1 0.0 copy-done.5
  10.2 0.0 copy-done.1
  10.2 0.0 copy-start.2
  10.2 1.2 %copy-done.2 = bf16[2,256,1024]{2,1,0:T(8,128)(2,1)S(1)} copy-done((bf16[2,256,1024]{2,1,0:T(8,128)(2,1)S(1)}, bf16[2,256,1024]{2,1,0:T(8,128)(2,1)}, u32[]{:S(2)}) %copy-start.2) | copy-done | bytes 1048600
  11.4 1.2 %copy-done.3 = bf16[2,512,512]{2,1,0:T(8,128)(2,1)S(1)} copy-done((bf16[2,512,512]{2,1,0:T(8,128)(2,1)S(1)}, bf16[2,512,512]{2,1,0:T(8,128)(2,1)}, u32[]{:S(2)}) %copy-start.3) | copy-done | bytes 1048600
  12.6 2.1 %shard_map.91.pack = bf16[1680,1024]{1,0:T(8,128)(2,1)} custom-call(bf16[1024,256]{1,0:T(8,128)(2,1)S(1)} %pad_maximum_fusion.after, bf16[2,256,1024]{2,1,0:T(8,128)(2,1)S(1)} %copy-done.1, bf16[2,256,1024]{2,1,0:T(8,128)(2,1)S(1)} %copy-done.2, bf16[2,512,512]{2,1,0:T(8,128)(2,1)S(1)} %copy-done.3, bf16[256,255]{1,0:T(8,128)(2,1)S(1)} %get-tuple-element.18.taps0, ...), custom_call_target="tpu_custom_call" | custom-call | flops 2000000000 | bytes 7000000 | tf_op jit(solution)/shard_map/pallas_call | solution.py:284
  14.8 2.3 %collective-permute-start.1 = (bf16[1680,1024]{1,0:T(8,128)(2,1)}, bf16[1680,1024]{1,0:T(8,128)(2,1)}, u32[]{:S(2)}, u32[]{:S(2)}) collective-permute-start(bf16[1680,1024]{1,0:T(8,128)(2,1)} %shard_map.91.pack), channel_id=1, source_target_pairs={{0,1},{1,0},{2,3},{3,2},{4,5},{5,4},{6,7},{7,6},{8,9},{9,8},{10,11... | collective-permute-start | bytes 10321928 | tf_op jit(solution)/shard_map/ppermute | solution.py:314
  17.1 1.9 %collective-permute-start = (bf16[1024,256]{1,0:T(8,128)(2,1)S(1)}, bf16[1024,256]{1,0:T(8,128)(2,1)S(1)}, u32[]{:S(2)}, u32[]{:S(2)}) collective-permute-start(bf16[1024,256]{1,0:T(8,128)(2,1)S(1)} %pad_maximum_fusion.after), channel_id=1, source_target_pairs={{1,2},{3,4},{5,6},{7,8},{9,10},{11,12},{13,14},{15,16},{17,18},{19... | collective-permute-start | bytes 1572872 | tf_op jit(solution)/shard_map/ppermute | solution.py:312
  19.0 0.1 pad_add_fusion.place
  19.1 4.2 %all-gather.1 = bf16[1024,256]{1,0:T(8,128)(2,1)S(1)} all-gather(bf16[512,256]{1,0:T(8,128)(2,1)S(1)} %get-tuple-element.15), channel_id=3, replica_groups=mesh['sp'=256,'tp'=2] {'tp'}, dimensions={0}, use_global_device_ids=true | all-gather | bytes 786432 | tf_op jit(solution)/shard_map/all_gather | solution.py:315
  23.3 4.2 %collective-permute-done.halo = bf16[1024,256]{1,0:T(8,128)(2,1)S(1)} collective-permute-done((bf16[1024,256]{1,0:T(8,128)(2,1)S(1)}, bf16[1024,256]{1,0:T(8,128)(2,1)S(1)}, u32[]{:S(2)}, u32[]{:S(2)}) %collective-permute-start) | collective-permute-done | bytes 524320 | tf_op jit(solution)/shard_map/ppermute | solution.py:312
  27.6 0.0 collective-permute-done.1.pack2
  27.6 0.0 copy-done.4
  27.6 0.0 copy-start.7
  27.6 1.6 %copy-done.7 = bf16[2048,512]{1,0:T(8,128)(2,1)S(1)} copy-done((bf16[2048,512]{1,0:T(8,128)(2,1)S(1)}, bf16[2048,512]{1,0:T(8,128)(2,1)}, u32[]{:S(2)}) %copy-start.7) | copy-done | bytes 2097176
  29.2 13.4 %shard_map.92 = (bf16[512,256]{1,0:T(8,128)(2,1)S(1)}, bf16[512,256]{1,0:T(8,128)(2,1)S(1)}) custom-call(s32[3]{0:T(128)S(1)} %pad_add_fusion.place, bf16[512,512]{1,0:T(8,128)(2,1)S(1)} %copy-done, bf16[2,512,256]{2,1,0:T(8,128)(2,1)S(1)} %bitcast.12, bf16[2,512,256]{2,1,0:T(8,128)(2,1)S(1)} %bitcast.13, bf16[1024,256]{1,0:T(8,128)(2,1)S(1)} %collective-permute-done.halo, ...), custom_call_target="tpu_custom_call" | custom-call | flops 7000000000 | bytes 10000000 | tf_op jit(solution)/shard_map/pallas_call | solution.py:220
  42.6 2.2 %all-gather.2 = bf16[1024,256]{1,0:T(8,128)(2,1)S(1)} all-gather(bf16[512,256]{1,0:T(8,128)(2,1)S(1)} %get-tuple-element.12), channel_id=4, replica_groups=mesh['sp'=256,'tp'=2] {'tp'}, dimensions={0}, use_global_device_ids=true | all-gather | bytes 786432 | tf_op jit(solution)/shard_map/all_gather | solution.py:324
  44.8 0.8 %pad_maximum_fusion.1 = bf16[512,512]{1,0:T(8,128)(2,1)} fusion(bf16[512,256]{1,0:T(8,128)(2,1)S(1)} %get-tuple-element.14, bf16[512,256]{1,0:T(8,128)(2,1)S(1)} %get-tuple-element.13), kind=kLoop, calls=%fused_computation.1 | loop fusion | flops 1048576 | bytes 1048576 | tf_op jit(solution)/shard_map/concatenate | solution.py:325
  (11 shorter events, 0.1 us)
Async XLA Ops:
  0.0 9.9 %copy-start.8 = (bf16[2,256,255]{1,0,2:T(2,128)(2,1)S(1)}, bf16[2,256,255]{1,0,2:T(2,128)(2,1)}, u32[]{:S(2)}) copy-start(bf16[2,256,255]{1,0,2:T(2,128)(2,1)} %param.13) | copy-start | bytes 783364
  0.0 10.1 %copy-start.6 = (f32[2,256]{1,0:T(2,128)S(1)}, f32[2,256]{1,0:T(2,128)}, u32[]{:S(2)}) copy-start(f32[2,256]{1,0:T(2,128)} %gshift.1) | copy-start | bytes 6148
  0.0 10.1 %copy-start.5 = (f32[2,256]{1,0:T(2,128)S(1)}, f32[2,256]{1,0:T(2,128)}, u32[]{:S(2)}) copy-start(f32[2,256]{1,0:T(2,128)} %ggain.1) | copy-start | bytes 6148
  0.0 10.1 %copy-start.1 = (bf16[2,256,1024]{2,1,0:T(8,128)(2,1)S(1)}, bf16[2,256,1024]{2,1,0:T(8,128)(2,1)}, u32[]{:S(2)}) copy-start(bf16[2,256,1024]{2,1,0:T(8,128)(2,1)} %wv.1) | copy-start | bytes 3145732
  10.2 1.2 %copy-start.2 = (bf16[2,256,1024]{2,1,0:T(8,128)(2,1)S(1)}, bf16[2,256,1024]{2,1,0:T(8,128)(2,1)}, u32[]{:S(2)}) copy-start(bf16[2,256,1024]{2,1,0:T(8,128)(2,1)} %wg.1) | copy-start | bytes 3145732
  11.4 1.2 %copy-start.3 = (bf16[2,512,512]{2,1,0:T(8,128)(2,1)S(1)}, bf16[2,512,512]{2,1,0:T(8,128)(2,1)}, u32[]{:S(2)}) copy-start(bf16[2,512,512]{2,1,0:T(8,128)(2,1)} %wo.1) | copy-start | bytes 3145732
  12.6 14.9 %copy-start = (bf16[512,512]{1,0:T(8,128)(2,1)S(1)}, bf16[512,512]{1,0:T(8,128)(2,1)}, u32[]{:S(2)}) copy-start(bf16[512,512]{1,0:T(8,128)(2,1)} %own.1) | copy-start | bytes 1572868
  12.6 14.9 %copy-start.4 = (f32[2,1024]{1,0:T(2,128)S(1)}, f32[2,1024]{1,0:T(2,128)}, u32[]{:S(2)}) copy-start(f32[2,1024]{1,0:T(2,128)} %gain.1) | copy-start | bytes 24580
  14.8 12.8 %collective-permute-start.1 = (bf16[1680,1024]{1,0:T(8,128)(2,1)}, bf16[1680,1024]{1,0:T(8,128)(2,1)}, u32[]{:S(2)}, u32[]{:S(2)}) collective-permute-start(bf16[1680,1024]{1,0:T(8,128)(2,1)} %shard_map.91.pack), channel_id=1, source_target_pairs={{0,1},{1,0},{2,3},{3,2},{4,5},{5,4},{6,7},{7,6},{8,9},{9,8},{10,11... | collective-permute-start | bytes 10321928 | tf_op jit(solution)/shard_map/ppermute | solution.py:314
  17.1 10.5 %collective-permute-start = (bf16[1024,256]{1,0:T(8,128)(2,1)S(1)}, bf16[1024,256]{1,0:T(8,128)(2,1)S(1)}, u32[]{:S(2)}, u32[]{:S(2)}) collective-permute-start(bf16[1024,256]{1,0:T(8,128)(2,1)S(1)} %pad_maximum_fusion.after), channel_id=1, source_target_pairs={{1,2},{3,4},{5,6},{7,8},{9,10},{11,12},{13,14},{15,16},{17,18},{19... | collective-permute-start | bytes 1572872 | tf_op jit(solution)/shard_map/ppermute | solution.py:312
  27.6 1.6 %copy-start.7 = (bf16[2048,512]{1,0:T(8,128)(2,1)S(1)}, bf16[2048,512]{1,0:T(8,128)(2,1)}, u32[]{:S(2)}) copy-start(bf16[2048,512]{1,0:T(8,128)(2,1)} %constant.26.clone.tables) | copy-start | bytes 6291460

commit v3 on v1

v3 whole, which is shorter than its diff:
```python
import functools

import jax
import jax.numpy as jnp
import numpy as np
from jax import lax
from jax.experimental import pallas as pl
from jax.experimental.pallas import tpu as pltpu
from jax.sharding import PartitionSpec as P


RMS_EPS = 1e-06
LN_EPS = 1e-05

WINDOW = 512
KEPT = 256
FIRST = 128
BINS = WINDOW // 2
HALF = 256
GATE_ROW = 256
OUT_ROW = 512
TAP_ROW = 768
GAIN_ROW = 896
OUTER_ROW = 912


def transform_tables(taps):
    bins = 2 * np.arange(BINS) + 1
    reach = (taps - 1) // 2

    def angles(left, right):
        return np.pi * (np.outer(left, right) % (2 * WINDOW)) / WINDOW

    time = angles(np.arange(WINDOW), bins)
    lag = angles(np.arange(taps) - reach, bins)
    back = angles(bins, np.arange(FIRST, FIRST + KEPT))
    tap_side = np.concatenate([np.cos(lag), np.sin(lag)], 1) * (2.0 / WINDOW)
    tap_side = np.pad(tap_side, ((0, 256 - taps), (0, 0)))
    forward = np.concatenate([np.cos(time), -np.sin(time)], 1)
    inverse = np.concatenate([np.cos(back), -np.sin(back)], 0)

    def terms(table):
        high = table.astype(jnp.bfloat16)
        return high, (table - high.astype(np.float64)).astype(jnp.bfloat16)

    return np.concatenate(
        [*terms(tap_side), *terms(forward), np.concatenate(terms(inverse), 1)], 0
    )


def dot(a, b):
    return jnp.dot(a, b, preferred_element_type=jnp.float32)


def column(row):
    return jnp.transpose(jnp.broadcast_to(row, (128, 128)))


def wide(col):
    return jnp.concatenate([col, col], 1)


def sigmoid(value):
    return 0.5 * jnp.tanh(0.5 * value) + 0.5


def lanes(block, size=HALF):
    return pl.ds(pl.multiple_of(block * size, size), size)


def norm_tile(source, cols, gains, layer, store):
    total = jnp.zeros((8, HALF), jnp.float32)
    for r in range(0, 1024, 128):
        piece = source[r : r + 128, cols].astype(jnp.float32)
        square = piece * piece
        for s in range(0, 128, 8):
            total += square[s : s + 8]
    mean = jnp.sum(total, axis=0, keepdims=True) * (1.0 / 1024.0)
    inverse = lax.rsqrt(mean + RMS_EPS)
    for j in range(8):
        r = slice(j * 128, (j + 1) * 128)
        piece = source[r, cols].astype(jnp.float32)
        store[r, :] = (piece * inverse * wide(gains[layer, r])).astype(jnp.bfloat16)


def project_tile(source, tokens, me):
    def product(start):
        r = slice(start, start + 256)
        total = dot(source[r, lanes(me, 512)], tokens[:512])
        total = total + dot(source[r, lanes(1 - me, 512)], tokens[512:])
        return total.astype(jnp.bfloat16).astype(jnp.float32)

    return (product(0) * sigmoid(product(GATE_ROW))).astype(jnp.bfloat16)


def branch(source, half, activated, me):
    r = slice(OUT_ROW, OUT_ROW + 256)
    total = dot(source[r, lanes(2 * half + me)], activated[:256])
    return total + dot(source[r, lanes(2 * half + 1 - me)], activated[256:])


def make_bins(source, layer, part, table):
    lane = (2 * layer + part) * 256
    taps = source[TAP_ROW : TAP_ROW + 128, lane : lane + 256]
    return dot(taps, table[:256]) + dot(taps, table[256:512])


def filter_norm(piece_of, bins, gcols, table, target):
    for chunk in range(2):
        piece = piece_of(slice(chunk * 256, (chunk + 1) * 256))
        freq = dot(piece, table[512:1024]) + dot(piece, table[1024:1536])
        re, im = freq[:, :BINS], freq[:, BINS:]
        tap_re, tap_im = bins[chunk][:, :BINS], bins[chunk][:, BINS:]
        prod = jnp.concatenate([re * tap_re - im * tap_im, re * tap_im + im * tap_re], 1)
        high = prod.astype(jnp.bfloat16)
        low = (prod - high.astype(jnp.float32)).astype(jnp.bfloat16)
        ih, il = table[1536:2048, :KEPT], table[1536:2048, KEPT:]
        filtered = dot(high, ih) + dot(low, ih) + dot(high, il)
        for g in range(2):
            v = filtered[g * 128 : (g + 1) * 128]
            c = slice(chunk * 256 + g * 128, chunk * 256 + (g + 1) * 128)
            centred = v - jnp.mean(v, axis=0, keepdims=True)
            var = jnp.mean(centred * centred, axis=0, keepdims=True)
            scaled = centred * lax.rsqrt(var + LN_EPS)
            scaled = scaled * wide(gcols[0, c]) + wide(gcols[1, c])
            target[c, :] = (scaled * sigmoid(scaled)).astype(jnp.bfloat16)


def group_columns(packs, layer, gcols):
    for chunk, source in enumerate(packs):
        terms = source[GAIN_ROW : GAIN_ROW + 16, :256].astype(jnp.float32)
        for g in range(2):
            for kind in range(2):
                t = terms[:, g * 128 : (g + 1) * 128]
                i = 6 * layer + 3 * kind
                row = t[i : i + 1] + t[i + 1 : i + 2] + t[i + 2 : i + 3]
                start = chunk * 256 + g * 128
                gcols[kind, start : start + 128] = column(row)


def early_kernel(tokens, gain, pack, table, normed, gated, bins, gains):
    me = lax.axis_index("tp")
    other = 1 - me
    for layer in range(2):
        for half, side in enumerate((me, other)):
            for j in range(4):
                row = gain[layer : layer + 1, lanes(4 * side + j, 128)]
                start = half * 512 + j * 128
                gains[layer, start : start + 128] = column(row)
    norm_tile(tokens, slice(0, HALF), gains, 0, normed)
    for layer in range(2):
        for part in range(2):
            bins[layer, part * 128 : (part + 1) * 128] = make_bins(pack, layer, part, table)
    gated[...] = project_tile(pack, normed, me)


def first_kernel(
    tokens, normed, gated_own, bins, gains, inner, halo, pack, pack2, table, x1, normed2,
    xw, normed1, gated, act, bins2, gcols,
):
    me = lax.axis_index("tp")
    block = lax.axis_index("sp")
    other = 1 - me
    packs = (pack, pack2)

    def stored(tile):
        return lanes(tile * me + (2 - tile) * other)

    xw[:512, :256] = inner[...]
    for q in range(4):
        r = slice(512 + 128 * q, 512 + 128 * (q + 1))
        xw[r, :256] = pack2[OUTER_ROW : OUTER_ROW + 128, 256 * q : 256 * (q + 1)]
    xw[:512, 512:] = halo[512:]
    xw[512:, 512:] = halo[:512]
    xw[:, 256:512] = tokens[...]
    for slot, tile in enumerate((0, 2)):
        cols = slice(tile * HALF, (tile + 1) * HALF)
        norm_tile(xw, cols, gains, 0, normed1.at[slot])
    group_columns(packs, 0, gcols)
    for part in range(2):
        bins2[part * 128 : (part + 1) * 128] = make_bins(pack2, 0, part, table)
    gated[:256, 256:512] = gated_own[...]
    gated[256:, 256:512] = project_tile(pack2, normed, me)
    for slot, tile in enumerate((0, 2)):
        cols = slice(tile * HALF, (tile + 1) * HALF)
        for chunk, source in enumerate(packs):
            r = slice(chunk * 256, (chunk + 1) * 256)
            gated[r, cols] = project_tile(source, normed1.at[slot], me)

    lane = lax.broadcasted_iota(jnp.int32, (8, KEPT), 1)
    ends = lax.axis_size("sp") - 1
    outside = (
        (lane < FIRST) & ((me == 0) & (block == 0)),
        (lane >= KEPT - FIRST) & ((me == 1) & (block == ends)),
    )

    def piece(b):
        return lambda r: jnp.concatenate([gated[r, stored(b)], gated[r, stored(b + 1)]], 1)

    def finish(b):
        for half, source in enumerate(packs):
            for part in range(2):
                start = half * 512 + part * 256
                r = slice(start, start + 256)
                before = jnp.concatenate(
                    [xw[r, stored(b)][:, FIRST:], xw[r, stored(b + 1)][:, :FIRST]], 1
                )
                total = before.astype(jnp.float32) + branch(source, part, act[b], me)
                drop = jnp.broadcast_to(outside[b][:1], total.shape)
                total = jnp.where(drop, 0.0, total)
                x1[r, b * KEPT : (b + 1) * KEPT] = total.astype(jnp.bfloat16)

    own = bins[0], bins2[...]
    filter_norm(piece(0), own, gcols, table, act.at[0])
    finish(0)
    filter_norm(piece(1), own, gcols, table, act.at[1])
    norm_tile(x1, slice(0, 256), gains, 1, normed2.at[0])
    finish(1)
    norm_tile(x1, slice(256, 512), gains, 1, normed2.at[1])


def second_kernel(
    x1, normed2, bins, pack, pack2, late, late2, table, keep, send, gated, act, bins2, gcols
):
    me = lax.axis_index("tp")
    group_columns((pack, pack2), 1, gcols)
    for part in range(2):
        bins2[part * 128 : (part + 1) * 128] = make_bins(pack2, 1, part, table)
    for tile in range(2):
        for chunk, source in enumerate((late, late2)):
            r = slice(chunk * 256, (chunk + 1) * 256)
            cols = slice(tile * HALF, (tile + 1) * HALF)
            gated[r, cols] = project_tile(source, normed2.at[tile], me)
    filter_norm(lambda r: gated[r, :], (bins[1], bins2[...]), gcols, table, act)
    cols = slice(FIRST, FIRST + KEPT)
    for half, (source, out) in enumerate(((late, keep), (late2, send))):
        for part in range(2):
            start = half * 512 + part * 256
            before = x1[start : start + 256, cols].astype(jnp.float32)
            total = before + branch(source, part, act, me)
            out[part * 256 : (part + 1) * 256] = total.astype(jnp.bfloat16)


def weight_copies(layer, wv, wg, wo, out, sems):
    copies = [
        (wv.at[layer], out.at[pl.ds(0, 256)]),
        (wg.at[layer], out.at[pl.ds(GATE_ROW, 256)]),
    ]
    for part in range(2):
        rows = pl.ds(256 * part, 256)
        copies.append((wo.at[layer, rows], out.at[pl.ds(OUT_ROW, 256), pl.ds(512 * part, 512)]))
    copies = [pltpu.make_async_copy(a, b, sems.at[i]) for i, (a, b) in enumerate(copies)]
    for copy in copies:
        copy.start()
    return copies


def pack_kernel(after, wv, wg, wo, taps0, taps1, ggain, gshift, outer, out, turned, sems):
    copies = weight_copies(0, wv, wg, wo, out, sems)
    for layer, taps in enumerate((taps0, taps1)):
        count = taps.shape[0]
        turned[:count] = taps[...].astype(jnp.float32)
        turned[count:] = jnp.zeros((256 - count, 256), jnp.float32)
        piece = jnp.transpose(turned[...]).astype(jnp.bfloat16)
        for chunk in range(2):
            lane = (2 * layer + chunk) * 256
            out[TAP_ROW : TAP_ROW + 128, lane : lane + 256] = piece[
                chunk * 128 : (chunk + 1) * 128
            ]
    for q in range(4):
        out[OUTER_ROW : OUTER_ROW + 128, 256 * q : 256 * (q + 1)] = outer[
            128 * q : 128 * (q + 1)
        ]
    rows = []
    for layer in range(2):
        for source in (ggain, gshift):
            rest = source[layer : layer + 1]
            for _ in range(3):
                term = rest.astype(jnp.bfloat16).astype(jnp.float32)
                rows.append(term)
                rest = rest - term
    rows.append(jnp.zeros((4, 256), jnp.float32))
    rows = jnp.concatenate(rows, 0).astype(jnp.bfloat16)
    out[GAIN_ROW:OUTER_ROW, :] = jnp.concatenate([rows, rows, rows, rows], 1)
    for copy in copies:
        copy.wait()


def late_pack_kernel(after, wv, wg, wo, out, sems):
    for copy in weight_copies(1, wv, wg, wo, out, sems):
        copy.wait()


def call(kernel, arrays, outs, scratch, limit, flops, unread=0, hbm=0):
    vmem = pl.BlockSpec(memory_space=pltpu.VMEM)
    specs = [pl.BlockSpec(memory_space=pl.ANY)] * unread
    specs += [pl.BlockSpec(memory_space=pltpu.HBM)] * hbm
    specs += [vmem] * (len(arrays) - unread - hbm)
    outs = [jax.ShapeDtypeStruct(shape, kind) for shape, kind in outs]
    return pl.pallas_call(
        kernel,
        out_shape=outs,
        in_specs=specs,
        out_specs=[vmem] * len(outs),
        scratch_shapes=scratch,
        compiler_params=pltpu.CompilerParams(vmem_limit_bytes=limit << 20),
        cost_estimate=pl.CostEstimate(
            flops=flops, bytes_accessed=4 * 10**6, transcendentals=2 * 10**5
        ),
    )(*arrays)


def body(blocks, stream, norm_gain, w_value, w_gate, conv_taps, group_gain, group_shift, w_out):
    taps = conv_taps.shape[2]
    me = lax.axis_index("tp")
    both = ("sp", "tp")
    partner = [(i, i ^ 1) for i in range(2 * blocks)]
    outward = [(2 * s + 1, 2 * s + 2) for s in range(blocks - 1)]
    outward += [(2 * s + 2, 2 * s + 1) for s in range(blocks - 1)]

    bf16, f32 = jnp.bfloat16, jnp.float32
    is_first = me == 0
    head, tail = stream[:, :HALF], stream[:, HALF:]
    outer = jnp.where(is_first, head, tail)
    inner = jnp.where(is_first, tail, head)
    inner, is_first = lax.optimization_barrier((inner, is_first))
    near = lax.all_gather(inner, "tp", axis=0)
    mine = jnp.concatenate([outer, jnp.where(is_first, near[1], near[0])], 0)
    tables = jnp.asarray(transform_tables(taps))
    mine, conv_taps = lax.optimization_barrier((mine, conv_taps))
    weights = [w_value, w_gate, w_out]
    halo = lax.ppermute(mine, both, outward)
    turned = [jnp.transpose(conv_taps[layer]) for layer in range(2)]
    (pack,) = call(
        pack_kernel,
        [mine, *weights, *turned, group_gain, group_shift, outer],
        [((OUTER_ROW + 128, 1024), bf16)],
        [pltpu.VMEM((256, 256), f32), pltpu.SemaphoreType.DMA((4,))],
        8, 2 * 10**9, 1, 3,
    )
    pack2 = lax.ppermute(pack, both, partner)
    (late,) = call(
        late_pack_kernel, [pack, *weights], [((TAP_ROW, 1024), bf16)],
        [pltpu.SemaphoreType.DMA((4,))], 4, 10**9, 1, 3,
    )
    late2 = lax.ppermute(late, both, partner)
    normed, gated, bins, gains = call(
        early_kernel,
        [mine, norm_gain, pack, tables],
        [
            ((1024, HALF), bf16), ((256, HALF), bf16),
            ((2, 256, WINDOW), f32), ((2, 1024, 128), f32),
        ],
        [], 12, 10**9,
    )
    x1, normed2 = call(
        first_kernel,
        [mine, normed, gated, bins, gains, inner, halo, pack, pack2, tables],
        [((1024, 512), bf16), ((2, 1024, HALF), bf16)],
        [
            pltpu.VMEM((1024, 768), bf16),
            pltpu.VMEM((2, 1024, HALF), bf16),
            pltpu.VMEM((512, 768), bf16),
            pltpu.VMEM((2, 512, KEPT), bf16),
            pltpu.VMEM((256, WINDOW), f32),
            pltpu.VMEM((2, 512, 128), f32),
        ],
        16, 4 * 10**9,
    )
    keep, send = call(
        second_kernel,
        [x1, normed2, bins, pack, pack2, late, late2, tables],
        [((512, KEPT), bf16), ((512, KEPT), bf16)],
        [
            pltpu.VMEM((512, 512), bf16),
            pltpu.VMEM((512, KEPT), bf16),
            pltpu.VMEM((256, WINDOW), f32),
            pltpu.VMEM((2, 512, 128), f32),
        ],
        12, 3 * 10**9,
    )
    swapped = lax.all_gather(send, "tp", axis=0)
    return jnp.concatenate(
        [jnp.where(is_first, keep, swapped[0]), jnp.where(is_first, swapped[1], keep)], 1
    )


def solution(mesh):
    placed = (
        P("tp", "sp"),
        P(),
        P(None, "tp", None),
        P(None, "tp", None),
        P(None, "tp", None),
        P(None, "tp"),
        P(None, "tp"),
        P(None, "tp", None),
    )
    return jax.shard_map(
        functools.partial(body, mesh.shape["sp"]),
        mesh=mesh, in_specs=placed, out_specs=P("tp", "sp"), check_vma=False,
    )
```

time: 79 us -> 38.5 us (0.49)
  the two profiles are of different devices: /device:TPU:385 before, /device:TPU:1 now
where the time goes in v3:
time: 38.5 us; the launch traced here: 38.3 us
  blocking collectives  11 us (29%)
  Pallas kernels  10.7 us (28%)
  waiting for transfers between devices  7.8 us (20%)
  starting transfers between devices  6.38 us (17%)
  other arithmetic  2.06 us (5%)
    pallas_call x5, Pallas kernels, call(): pl.pallas_call(kernel, out_shape=outs, in_specs=specs, out_specs=[vmem] *...  10.7 us
    all_gather x1, blocking collectives, body(): near = lax.all_gather(inner, 'tp', axis=0)  8.78 us
    ppermute x1, waiting for transfers between devices, body(): halo = lax.ppermute(mine, both, outward)  7.8 us
    ppermute x1, starting transfers between devices, body(): pack2 = lax.ppermute(pack, both, partner)  2.41 us
    all_gather x1, blocking collectives, body(): swapped = lax.all_gather(send, 'tp', axis=0)  2.18 us
    ppermute x1, starting transfers between devices, body(): late2 = lax.ppermute(late, both, partner)  2.04 us
    ppermute x1, starting transfers between devices, body(): halo = lax.ppermute(mine, both, outward)  1.92 us
    select_n x1, other arithmetic, body(): outer = jnp.where(is_first, head, tail)  1.11 us
  transfers between devices with their start and end apart: 3, of which 1 were waited for; matrix products, arithmetic and copies ran while one was open for 0% of the time, Pallas kernels for 18%

profile of v3, /device:TPU:1, one launch (start us, length us, event | category | flops | bytes accessed | tf_op | source)
XLA Modules:
  0.0 38.3 jit_solution(2133298509527273939)
XLA Ops:
  0.0 1.1 %broadcast_select_fusion = (bf16[512,256]{1,0:T(8,128)(2,1)S(1)}, bf16[512,256]{1,0:T(8,128)(2,1)S(1)}) fusion(pred[]{:T(512)S(6)} %eq.3, bf16[512,512]{1,0:T(8,128)(2,1)} %param.9), kind=kLoop, calls=%fused_computation.5 | loop fusion | flops 262144 | bytes 1048577 | tf_op jit(solution)/shard_map/jit(_where)/select_n | solution.py:324
  1.1 0.0 copy-start.1
  1.1 0.0 copy-start.2
  1.1 0.0 copy-start.3
  1.2 0.0 copy-start.5
  1.2 0.0 copy-start.6
  1.2 8.8 %all-gather = bf16[1024,256]{1,0:T(8,128)(2,1)S(1)} all-gather(bf16[512,256]{1,0:T(8,128)(2,1)S(1)} %get-tuple-element.18.inner), channel_id=2, replica_groups=mesh['sp'=256,'tp'=2] {'tp'}, dimensions={0}, use_global_device_ids=true | all-gather | bytes 786432 | tf_op jit(solution)/shard_map/all_gather | solution.py:327
  10.0 0.0 copy-done.7
  10.2 0.3 shard_map.91.pack.after
  10.5 0.0 copy-start
  10.5 0.0 copy-start.4
  10.5 2.4 %collective-permute-start.1 = (bf16[1040,1024]{1,0:T(8,128)(2,1)S(1)}, bf16[1040,1024]{1,0:T(8,128)(2,1)S(1)}, u32[]{:S(2)}, u32[]{:S(2)}) collective-permute-start(bf16[1040,1024]{1,0:T(8,128)(2,1)S(1)} %shard_map.91.pack.after), channel_id=1, source_target_pairs={{0,1},{1,0},{2,3},{3,2},{4,5},{5,4},{6,7},{7,6},{8,9},{9,8},{10,11... | collective-permute-start | bytes 6389768 | tf_op jit(solution)/shard_map/ppermute | solution.py:341
  12.9 0.2 shard_map.94.late
  13.1 2.0 %collective-permute-start.2 = (bf16[768,1024]{1,0:T(8,128)(2,1)S(1)}, bf16[768,1024]{1,0:T(8,128)(2,1)S(1)}, u32[]{:S(2)}, u32[]{:S(2)}) collective-permute-start(bf16[768,1024]{1,0:T(8,128)(2,1)S(1)} %shard_map.94.late), channel_id=1, source_target_pairs={{0,1},{1,0},{2,3},{3,2},{4,5},{5,4},{6,7},{7,6},{8,9},{9,8},{10,11... | collective-permute-start | bytes 4718600 | tf_op jit(solution)/shard_map/ppermute | solution.py:346
  15.1 1.9 %collective-permute-start = (bf16[1024,256]{1,0:T(8,128)(2,1)S(1)}, bf16[1024,256]{1,0:T(8,128)(2,1)S(1)}, u32[]{:S(2)}, u32[]{:S(2)}) collective-permute-start(bf16[1024,256]{1,0:T(8,128)(2,1)S(1)} %pad_maximum_fusion.after.tokens), channel_id=1, source_target_pairs={{1,2},{3,4},{5,6},{7,8},{9,10},{11,12},{13,14},{15,16},{17,18},{19... | collective-permute-start | bytes 1572872 | tf_op jit(solution)/shard_map/ppermute | solution.py:332
  17.1 0.7 %shard_map.92 = (bf16[1024,256]{1,0:T(8,128)(2,1)S(1)}, bf16[256,256]{1,0:T(8,128)(2,1)S(1)}, f32[2,256,512]{2,1,0:T(8,128)S(1)}, f32[2,1024,128]{2,1,0:T(8,128)S(1)}) custom-call(bf16[1024,256]{1,0:T(8,128)(2,1)S(1)} %pad_maximum_fusion.after.tokens, f32[2,1024]{1,0:T(2,128)S(1)} %copy-done.4, bf16[1040,1024]{1,0:T(8,128)(2,1)S(1)} %shard_map.91.pack.after, ...), custom_call_target="tpu_custom_call" | custom-call | flops 1000000000 | bytes 4000000 | tf_op jit(solution)/shard_map/pallas_call | solution.py:300
  17.8 7.8 %collective-permute-done.halo = bf16[1024,256]{1,0:T(8,128)(2,1)S(1)} collective-permute-done((bf16[1024,256]{1,0:T(8,128)(2,1)S(1)}, bf16[1024,256]{1,0:T(8,128)(2,1)S(1)}, u32[]{:S(2)}, u32[]{:S(2)}) %collective-permute-start) | collective-permute-done | bytes 524320 | tf_op jit(solution)/shard_map/ppermute | solution.py:332
  25.6 0.0 collective-permute-done.1.pack2
  25.6 6.1 %shard_map.93 = (bf16[1024,512]{1,0:T(8,128)(2,1)S(1)}, bf16[2,1024,256]{2,1,0:T(8,128)(2,1)S(1)}) custom-call(bf16[1024,256]{1,0:T(8,128)(2,1)S(1)} %pad_maximum_fusion.after.tokens, bf16[1024,256]{1,0:T(8,128)(2,1)S(1)} %get-tuple-element.21.normed, bf16[256,256]{1,0:T(8,128)(2,1)S(1)} %get-tuple-element.22.gated_own, ...), custom_call_target="tpu_custom_call" | custom-call | flops 4000000000 | bytes 4000000 | tf_op jit(solution)/shard_map/pallas_call | solution.py:300
  31.7 0.0 collective-permute-done.2.late2
  31.7 3.5 %shard_map.95 = (bf16[512,256]{1,0:T(8,128)(2,1)S(1)}, bf16[512,256]{1,0:T(8,128)(2,1)S(1)}) custom-call(bf16[1024,512]{1,0:T(8,128)(2,1)S(1)} %get-tuple-element.25.x1, bf16[2,1024,256]{2,1,0:T(8,128)(2,1)S(1)} %get-tuple-element.26.normed2, f32[2,256,512]{2,1,0:T(8,128)S(1)} %get-tuple-element.23.bins, bf16[1040,1024]{1,0:T(8,128)(2,1)S(1)} %shard_map.91.pack.after, ...), custom_call_target="tpu_custom_call" | custom-call | flops 3000000000 | bytes 4000000 | tf_op jit(solution)/shard_map/pallas_call | solution.py:300
  35.2 2.2 %all-gather.1 = bf16[1024,256]{1,0:T(8,128)(2,1)S(1)} all-gather(bf16[512,256]{1,0:T(8,128)(2,1)S(1)} %get-tuple-element.28), channel_id=3, replica_groups=mesh['sp'=256,'tp'=2] {'tp'}, dimensions={0}, use_global_device_ids=true | all-gather | bytes 786432 | tf_op jit(solution)/shard_map/all_gather | solution.py:382
  37.4 0.1 slice_select_fusion.1
  37.4 0.8 %pad_maximum_fusion.1 = bf16[512,512]{1,0:T(8,128)(2,1)} fusion(bf16[512,256]{1,0:T(8,128)(2,1)S(1)} %get-tuple-element.30, bf16[512,256]{1,0:T(8,128)(2,1)S(1)} %get-tuple-element.29), kind=kLoop, calls=%fused_computation.1 | loop fusion | flops 1048576 | bytes 1048576 | tf_op jit(solution)/shard_map/concatenate | solution.py:383
  (12 shorter events, 0.1 us)
Async XLA Ops:
  0.0 10.0 %copy-start.7 = (bf16[2,256,255]{1,0,2:T(2,128)(2,1)S(1)}, bf16[2,256,255]{1,0,2:T(2,128)(2,1)}, u32[]{:S(2)}) copy-start(bf16[2,256,255]{1,0,2:T(2,128)(2,1)} %param.13) | copy-start | bytes 783364
  1.1 9.0 %copy-start.1 = (bf16[2,256,1024]{2,1,0:T(8,128)(2,1)S(1)}, bf16[2,256,1024]{2,1,0:T(8,128)(2,1)}, u32[]{:S(2)}) copy-start(bf16[2,256,1024]{2,1,0:T(8,128)(2,1)} %wv.3) | copy-start | bytes 3145732
  1.1 9.0 %copy-start.2 = (bf16[2,256,1024]{2,1,0:T(8,128)(2,1)S(1)}, bf16[2,256,1024]{2,1,0:T(8,128)(2,1)}, u32[]{:S(2)}) copy-start(bf16[2,256,1024]{2,1,0:T(8,128)(2,1)} %wg.3) | copy-start | bytes 3145732
  1.1 9.0 %copy-start.3 = (bf16[2,512,512]{2,1,0:T(8,128)(2,1)S(1)}, bf16[2,512,512]{2,1,0:T(8,128)(2,1)}, u32[]{:S(2)}) copy-start(bf16[2,512,512]{2,1,0:T(8,128)(2,1)} %wo.3) | copy-start | bytes 3145732
  1.2 9.0 %copy-start.5 = (f32[2,256]{1,0:T(2,128)S(1)}, f32[2,256]{1,0:T(2,128)}, u32[]{:S(2)}) copy-start(f32[2,256]{1,0:T(2,128)} %ggain.1) | copy-start | bytes 6148
  1.2 9.0 %copy-start.6 = (f32[2,256]{1,0:T(2,128)S(1)}, f32[2,256]{1,0:T(2,128)}, u32[]{:S(2)}) copy-start(f32[2,256]{1,0:T(2,128)} %gshift.1) | copy-start | bytes 6148
  10.5 6.6 %copy-start = (bf16[2048,512]{1,0:T(8,128)(2,1)S(1)}, bf16[2048,512]{1,0:T(8,128)(2,1)}, u32[]{:S(2)}) copy-start(bf16[2048,512]{1,0:T(8,128)(2,1)} %constant.8.clone.table) | copy-start | bytes 6291460
  10.5 6.6 %copy-start.4 = (f32[2,1024]{1,0:T(2,128)S(1)}, f32[2,1024]{1,0:T(2,128)}, u32[]{:S(2)}) copy-start(f32[2,1024]{1,0:T(2,128)} %gain.1) | copy-start | bytes 24580
  10.5 15.1 %collective-permute-start.1 = (bf16[1040,1024]{1,0:T(8,128)(2,1)S(1)}, bf16[1040,1024]{1,0:T(8,128)(2,1)S(1)}, u32[]{:S(2)}, u32[]{:S(2)}) collective-permute-start(bf16[1040,1024]{1,0:T(8,128)(2,1)S(1)} %shard_map.91.pack.after), channel_id=1, source_target_pairs={{0,1},{1,0},{2,3},{3,2},{4,5},{5,4},{6,7},{7,6},{8,9},{9,8},{10,11... | collective-permute-start | bytes 6389768 | tf_op jit(solution)/shard_map/ppermute | solution.py:341
  13.1 18.6 %collective-permute-start.2 = (bf16[768,1024]{1,0:T(8,128)(2,1)S(1)}, bf16[768,1024]{1,0:T(8,128)(2,1)S(1)}, u32[]{:S(2)}, u32[]{:S(2)}) collective-permute-start(bf16[768,1024]{1,0:T(8,128)(2,1)S(1)} %shard_map.94.late), channel_id=1, source_target_pairs={{0,1},{1,0},{2,3},{3,2},{4,5},{5,4},{6,7},{7,6},{8,9},{9,8},{10,11... | collective-permute-start | bytes 4718600 | tf_op jit(solution)/shard_map/ppermute | solution.py:346
  15.1 10.5 %collective-permute-start = (bf16[1024,256]{1,0:T(8,128)(2,1)S(1)}, bf16[1024,256]{1,0:T(8,128)(2,1)S(1)}, u32[]{:S(2)}, u32[]{:S(2)}) collective-permute-start(bf16[1024,256]{1,0:T(8,128)(2,1)S(1)} %pad_maximum_fusion.after.tokens), channel_id=1, source_target_pairs={{1,2},{3,4},{5,6},{7,8},{9,10},{11,12},{13,14},{15,16},{17,18},{19... | collective-permute-start | bytes 1572872 | tf_op jit(solution)/shard_map/ppermute | solution.py:332

commit v4 on v3

--- a/solution.py
+++ b/solution.py
@@ -18,10 +18,12 @@
 BINS = WINDOW // 2
 HALF = 256
 GATE_ROW = 256
+TAP_ROW = 512
+GAIN_ROW = 640
+TOKEN_ROW = 656
+PACK_ROWS = 912
 OUT_ROW = 512
-TAP_ROW = 768
-GAIN_ROW = 896
-OUTER_ROW = 912
+LATE_ROWS = 1024
 
 
 def transform_tables(taps):
@@ -93,8 +95,8 @@
     return (product(0) * sigmoid(product(GATE_ROW))).astype(jnp.bfloat16)
 
 
-def branch(source, half, activated, me):
-    r = slice(OUT_ROW, OUT_ROW + 256)
+def branch(source, layer, half, activated, me):
+    r = slice(OUT_ROW + 256 * layer, OUT_ROW + 256 * (layer + 1))
     total = dot(source[r, lanes(2 * half + me)], activated[:256])
     return total + dot(source[r, lanes(2 * half + 1 - me)], activated[256:])
 
@@ -138,7 +140,20 @@
                 gcols[kind, start : start + 128] = column(row)
 
 
-def early_kernel(tokens, gain, pack, table, normed, gated, bins, gains):
+def split_kernel(stream, outer, inner):
+    me = lax.axis_index("tp")
+    outer[...] = stream[:, lanes(me)]
+    inner[...] = stream[:, lanes(1 - me)]
+
+
+def join_kernel(keep, swapped, out):
+    me = lax.axis_index("tp")
+    other = 1 - me
+    out[:, lanes(me)] = keep[...]
+    out[:, lanes(other)] = swapped[other]
+
+
+def early_kernel(gain, pack, table, bins, gains):
     me = lax.axis_index("tp")
     other = 1 - me
     for layer in range(2):
@@ -147,45 +162,63 @@
                 row = gain[layer : layer + 1, lanes(4 * side + j, 128)]
                 start = half * 512 + j * 128
                 gains[layer, start : start + 128] = column(row)
-    norm_tile(tokens, slice(0, HALF), gains, 0, normed)
     for layer in range(2):
         for part in range(2):
             bins[layer, part * 128 : (part + 1) * 128] = make_bins(pack, layer, part, table)
-    gated[...] = project_tile(pack, normed, me)
+
+
+def stored(tile, me):
+    return lanes(tile * me + (2 - tile) * (1 - me))
 
 
 def first_kernel(
-    tokens, normed, gated_own, bins, gains, inner, halo, pack, pack2, table, x1, normed2,
-    xw, normed1, gated, act, bins2, gcols,
+    bins, gains, inner, outer, halo_own, halo_other, pack, pack2, table, xw, act,
+    normed1, gated, bins2, gcols,
+):
+    me = lax.axis_index("tp")
+    packs = (pack, pack2)
+
+    xw[:512, :256] = inner[...]
+    xw[:512, 256:512] = outer[...]
+    for tile in range(2):
+        start = TOKEN_ROW + 128 * (1 - tile)
+        for q in range(4):
+            r = slice(512 + 128 * q, 512 + 128 * (q + 1))
+            xw[r, 256 * tile : 256 * (tile + 1)] = pack2[
+                start : start + 128, 256 * q : 256 * (q + 1)
+            ]
+    xw[:512, 512:] = halo_own[...]
+    xw[512:, 512:] = halo_other[...]
+    group_columns(packs, 0, gcols)
+
+    def project_all(tile):
+        cols = slice(tile * HALF, (tile + 1) * HALF)
+        for chunk, source in enumerate(packs):
+            r = slice(chunk * 256, (chunk + 1) * 256)
+            gated[r, cols] = project_tile(source, normed1.at[tile], me)
+
+    for tile in range(3):
+        norm_tile(xw, slice(tile * HALF, (tile + 1) * HALF), gains, 0, normed1.at[tile])
+        if tile:
+            project_all(tile - 1)
+    for part in range(2):
+        bins2[part * 128 : (part + 1) * 128] = make_bins(pack2, 0, part, table)
+    project_all(2)
+
+    def piece(b):
+        return lambda r: jnp.concatenate([gated[r, stored(b, me)], gated[r, stored(b + 1, me)]], 1)
+
+    own = bins[0], bins2[...]
+    for b in range(2):
+        filter_norm(piece(b), own, gcols, table, act.at[b])
+
+
+def second_kernel(
+    xw, act, bins, gains, pack, pack2, late, late2, table, keep, send,
+    x1, normed2, gated, act2, bins2, gcols,
 ):
     me = lax.axis_index("tp")
     block = lax.axis_index("sp")
-    other = 1 - me
-    packs = (pack, pack2)
-
-    def stored(tile):
-        return lanes(tile * me + (2 - tile) * other)
-
-    xw[:512, :256] = inner[...]
-    for q in range(4):
-        r = slice(512 + 128 * q, 512 + 128 * (q + 1))
-        xw[r, :256] = pack2[OUTER_ROW : OUTER_ROW + 128, 256 * q : 256 * (q + 1)]
-    xw[:512, 512:] = halo[512:]
-    xw[512:, 512:] = halo[:512]
-    xw[:, 256:512] = tokens[...]
-    for slot, tile in enumerate((0, 2)):
-        cols = slice(tile * HALF, (tile + 1) * HALF)
-        norm_tile(xw, cols, gains, 0, normed1.at[slot])
-    group_columns(packs, 0, gcols)
-    for part in range(2):
-        bins2[part * 128 : (part + 1) * 128] = make_bins(pack2, 0, part, table)
-    gated[:256, 256:512] = gated_own[...]
-    gated[256:, 256:512] = project_tile(pack2, normed, me)
-    for slot, tile in enumerate((0, 2)):
-        cols = slice(tile * HALF, (tile + 1) * HALF)
-        for chunk, source in enumerate(packs):
-            r = slice(chunk * 256, (chunk + 1) * 256)
-            gated[r, cols] = project_tile(source, normed1.at[slot], me)
 
     lane = lax.broadcasted_iota(jnp.int32, (8, KEPT), 1)
     ends = lax.axis_size("sp") - 1
@@ -194,69 +227,57 @@
         (lane >= KEPT - FIRST) & ((me == 1) & (block == ends)),
     )
 
-    def piece(b):
-        return lambda r: jnp.concatenate([gated[r, stored(b)], gated[r, stored(b + 1)]], 1)
-
     def finish(b):
-        for half, source in enumerate(packs):
+        for half, source in enumerate((late, late2)):
             for part in range(2):
                 start = half * 512 + part * 256
                 r = slice(start, start + 256)
                 before = jnp.concatenate(
-                    [xw[r, stored(b)][:, FIRST:], xw[r, stored(b + 1)][:, :FIRST]], 1
+                    [xw[r, stored(b, me)][:, FIRST:], xw[r, stored(b + 1, me)][:, :FIRST]], 1
                 )
-                total = before.astype(jnp.float32) + branch(source, part, act[b], me)
+                total = before.astype(jnp.float32) + branch(source, 0, part, act[b], me)
                 drop = jnp.broadcast_to(outside[b][:1], total.shape)
                 total = jnp.where(drop, 0.0, total)
                 x1[r, b * KEPT : (b + 1) * KEPT] = total.astype(jnp.bfloat16)
 
-    own = bins[0], bins2[...]
-    filter_norm(piece(0), own, gcols, table, act.at[0])
     finish(0)
-    filter_norm(piece(1), own, gcols, table, act.at[1])
     norm_tile(x1, slice(0, 256), gains, 1, normed2.at[0])
     finish(1)
-    norm_tile(x1, slice(256, 512), gains, 1, normed2.at[1])
-
-
-def second_kernel(
-    x1, normed2, bins, pack, pack2, late, late2, table, keep, send, gated, act, bins2, gcols
-):
-    me = lax.axis_index("tp")
     group_columns((pack, pack2), 1, gcols)
     for part in range(2):
         bins2[part * 128 : (part + 1) * 128] = make_bins(pack2, 1, part, table)
+    norm_tile(x1, slice(256, 512), gains, 1, normed2.at[1])
     for tile in range(2):
         for chunk, source in enumerate((late, late2)):
             r = slice(chunk * 256, (chunk + 1) * 256)
             cols = slice(tile * HALF, (tile + 1) * HALF)
             gated[r, cols] = project_tile(source, normed2.at[tile], me)
-    filter_norm(lambda r: gated[r, :], (bins[1], bins2[...]), gcols, table, act)
+    filter_norm(lambda r: gated[r, :], (bins[1], bins2[...]), gcols, table, act2)
     cols = slice(FIRST, FIRST + KEPT)
     for half, (source, out) in enumerate(((late, keep), (late2, send))):
         for part in range(2):
             start = half * 512 + part * 256
             before = x1[start : start + 256, cols].astype(jnp.float32)
-            total = before + branch(source, part, act, me)
+            total = before + branch(source, 1, part, act2, me)
             out[part * 256 : (part + 1) * 256] = total.astype(jnp.bfloat16)
 
 
-def weight_copies(layer, wv, wg, wo, out, sems):
-    copies = [
+def start_copies(pairs, sems):
+    copies = [pltpu.make_async_copy(a, b, sems.at[i]) for i, (a, b) in enumerate(pairs)]
+    for copy in copies:
+        copy.start()
+    return copies
+
+
+def in_weights(layer, wv, wg, out):
+    return [
         (wv.at[layer], out.at[pl.ds(0, 256)]),
         (wg.at[layer], out.at[pl.ds(GATE_ROW, 256)]),
     ]
-    for part in range(2):
-        rows = pl.ds(256 * part, 256)
-        copies.append((wo.at[layer, rows], out.at[pl.ds(OUT_ROW, 256), pl.ds(512 * part, 512)]))
-    copies = [pltpu.make_async_copy(a, b, sems.at[i]) for i, (a, b) in enumerate(copies)]
-    for copy in copies:
-        copy.start()
-    return copies
-
-
-def pack_kernel(after, wv, wg, wo, taps0, taps1, ggain, gshift, outer, out, turned, sems):
-    copies = weight_copies(0, wv, wg, wo, out, sems)
+
+
+def pack_kernel(wv, wg, taps0, taps1, ggain, gshift, inner, outer, out, turned, sems):
+    copies = start_copies(in_weights(0, wv, wg, out), sems)
     for layer, taps in enumerate((taps0, taps1)):
         count = taps.shape[0]
         turned[:count] = taps[...].astype(jnp.float32)
@@ -267,10 +288,10 @@
             out[TAP_ROW : TAP_ROW + 128, lane : lane + 256] = piece[
                 chunk * 128 : (chunk + 1) * 128
             ]
-    for q in range(4):
-        out[OUTER_ROW : OUTER_ROW + 128, 256 * q : 256 * (q + 1)] = outer[
-            128 * q : 128 * (q + 1)
-        ]
+    for half, tokens in enumerate((inner, outer)):
+        start = TOKEN_ROW + 128 * half
+        for q in range(4):
+            out[start : start + 128, 256 * q : 256 * (q + 1)] = tokens[128 * q : 128 * (q + 1)]
     rows = []
     for layer in range(2):
         for source in (ggain, gshift):
@@ -281,13 +302,18 @@
                 rest = rest - term
     rows.append(jnp.zeros((4, 256), jnp.float32))
     rows = jnp.concatenate(rows, 0).astype(jnp.bfloat16)
-    out[GAIN_ROW:OUTER_ROW, :] = jnp.concatenate([rows, rows, rows, rows], 1)
+    out[GAIN_ROW:TOKEN_ROW, :] = jnp.concatenate([rows, rows, rows, rows], 1)
     for copy in copies:
         copy.wait()
 
 
 def late_pack_kernel(after, wv, wg, wo, out, sems):
-    for copy in weight_copies(1, wv, wg, wo, out, sems):
+    pairs = in_weights(1, wv, wg, out)
+    for layer in range(2):
+        for part in range(2):
+            target = out.at[pl.ds(OUT_ROW + 256 * layer, 256), pl.ds(512 * part, 512)]
+            pairs.append((wo.at[layer, pl.ds(256 * part, 256)], target))
+    for copy in start_copies(pairs, sems):
         copy.wait()
 
 
@@ -312,56 +338,48 @@
 
 def body(blocks, stream, norm_gain, w_value, w_gate, conv_taps, group_gain, group_shift, w_out):
     taps = conv_taps.shape[2]
-    me = lax.axis_index("tp")
     both = ("sp", "tp")
     partner = [(i, i ^ 1) for i in range(2 * blocks)]
     outward = [(2 * s + 1, 2 * s + 2) for s in range(blocks - 1)]
     outward += [(2 * s + 2, 2 * s + 1) for s in range(blocks - 1)]
+    along = [(2 * s, 2 * s + 2) for s in range(blocks - 1)]
+    along += [(2 * s + 3, 2 * s + 1) for s in range(blocks - 1)]
 
     bf16, f32 = jnp.bfloat16, jnp.float32
-    is_first = me == 0
-    head, tail = stream[:, :HALF], stream[:, HALF:]
-    outer = jnp.where(is_first, head, tail)
-    inner = jnp.where(is_first, tail, head)
-    inner, is_first = lax.optimization_barrier((inner, is_first))
-    near = lax.all_gather(inner, "tp", axis=0)
-    mine = jnp.concatenate([outer, jnp.where(is_first, near[1], near[0])], 0)
+    half = ((512, HALF), bf16)
+    outer, inner = call(split_kernel, [stream], [half, half], [], 4, 2 * 10**10)
+    outer, inner, conv_taps = lax.optimization_barrier((outer, inner, conv_taps))
     tables = jnp.asarray(transform_tables(taps))
-    mine, conv_taps = lax.optimization_barrier((mine, conv_taps))
-    weights = [w_value, w_gate, w_out]
-    halo = lax.ppermute(mine, both, outward)
+    halo_other = lax.ppermute(outer, both, outward)
+    halo_own = lax.ppermute(inner, both, along)
     turned = [jnp.transpose(conv_taps[layer]) for layer in range(2)]
     (pack,) = call(
         pack_kernel,
-        [mine, *weights, *turned, group_gain, group_shift, outer],
-        [((OUTER_ROW + 128, 1024), bf16)],
-        [pltpu.VMEM((256, 256), f32), pltpu.SemaphoreType.DMA((4,))],
-        8, 2 * 10**9, 1, 3,
+        [w_value, w_gate, *turned, group_gain, group_shift, inner, outer],
+        [((PACK_ROWS, 1024), bf16)],
+        [pltpu.VMEM((256, 256), f32), pltpu.SemaphoreType.DMA((2,))],
+        8, 2 * 10**9, 0, 2,
     )
     pack2 = lax.ppermute(pack, both, partner)
     (late,) = call(
-        late_pack_kernel, [pack, *weights], [((TAP_ROW, 1024), bf16)],
-        [pltpu.SemaphoreType.DMA((4,))], 4, 10**9, 1, 3,
+        late_pack_kernel, [pack, w_value, w_gate, w_out],
+        [((LATE_ROWS, 1024), bf16)],
+        [pltpu.SemaphoreType.DMA((6,))], 4, 10**9, 1, 3,
     )
     late2 = lax.ppermute(late, both, partner)
-    normed, gated, bins, gains = call(
+    bins, gains = call(
         early_kernel,
-        [mine, norm_gain, pack, tables],
+        [norm_gain, pack, tables],
+        [((2, 256, WINDOW), f32), ((2, 1024, 128), f32)],
+        [], 12, 10**9,
+    )
+    xw, act = call(
+        first_kernel,
+        [bins, gains, inner, outer, halo_own, halo_other, pack, pack2, tables],
+        [((1024, 768), bf16), ((2, 512, KEPT), bf16)],
         [
-            ((1024, HALF), bf16), ((256, HALF), bf16),
-            ((2, 256, WINDOW), f32), ((2, 1024, 128), f32),
-        ],
-        [], 12, 10**9,
-    )
-    x1, normed2 = call(
-        first_kernel,
-        [mine, normed, gated, bins, gains, inner, halo, pack, pack2, tables],
-        [((1024, 512), bf16), ((2, 1024, HALF), bf16)],
-        [
-            pltpu.VMEM((1024, 768), bf16),
-            pltpu.VMEM((2, 1024, HALF), bf16),
+            pltpu.VMEM((3, 1024, HALF), bf16),
             pltpu.VMEM((512, 768), bf16),
-            pltpu.VMEM((2, 512, KEPT), bf16),
             pltpu.VMEM((256, WINDOW), f32),
             pltpu.VMEM((2, 512, 128), f32),
         ],
@@ -369,20 +387,20 @@
     )
     keep, send = call(
         second_kernel,
-        [x1, normed2, bins, pack, pack2, late, late2, tables],
+        [xw, act, bins, gains, pack, pack2, late, late2, tables],
         [((512, KEPT), bf16), ((512, KEPT), bf16)],
         [
+            pltpu.VMEM((1024, 512), bf16),
+            pltpu.VMEM((2, 1024, HALF), bf16),
             pltpu.VMEM((512, 512), bf16),
             pltpu.VMEM((512, KEPT), bf16),
             pltpu.VMEM((256, WINDOW), f32),
             pltpu.VMEM((2, 512, 128), f32),
         ],
-        12, 3 * 10**9,
+        16, 3 * 10**9,
     )
     swapped = lax.all_gather(send, "tp", axis=0)
-    return jnp.concatenate(
-        [jnp.where(is_first, keep, swapped[0]), jnp.where(is_first, swapped[1], keep)], 1
-    )
+    return call(join_kernel, [keep, swapped], [((512, 512), bf16)], [], 4, 10**8)[0]
 
 
 def solution(mesh):

time: 38.5 us -> 36.5 us (0.948)
  the two profiles are of different devices: /device:TPU:1 before, /device:TPU:385 now
where the time goes in v4:
time: 36.5 us; the launch traced here: 36.3 us
  starting transfers between devices  15 us (41%)
  Pallas kernels  11 us (30%)
  waiting for transfers between devices  5.58 us (15%)
  blocking collectives  2.34 us (6%)
  local copies, waits for them, and re-layouts  2.18 us (6%)
    pallas_call x7, Pallas kernels, call(): pl.pallas_call(kernel, out_shape=outs, in_specs=specs, out_specs=[vmem] *...  11 us
    ppermute x1, starting transfers between devices, body(): halo_own = lax.ppermute(inner, both, along)  8.49 us
    ppermute x1, waiting for transfers between devices, body(): halo_other = lax.ppermute(outer, both, outward)  4.69 us
    ppermute x1, starting transfers between devices, body(): pack2 = lax.ppermute(pack, both, partner)  2.72 us
    all_gather x1, blocking collectives, body(): swapped = lax.all_gather(send, 'tp', axis=0)  2.34 us
    unnamed x18, local copies, waits for them, and re-layouts  2.13 us
    ppermute x1, starting transfers between devices, body(): late2 = lax.ppermute(late, both, partner)  1.92 us
    ppermute x1, starting transfers between devices, body(): halo_other = lax.ppermute(outer, both, outward)  1.92 us
  transfers between devices with their start and end apart: 4, of which 2 were waited for; matrix products, arithmetic and copies ran while one was open for 0% of the time, Pallas kernels for 16%

profile of v4, /device:TPU:385, one launch (start us, length us, event | category | flops | bytes accessed | tf_op | source)
XLA Modules:
  0.0 36.3 jit_solution(3434015601015840850)
XLA Ops:
  0.0 1.2 %copy-done.5 = bf16[512,512]{1,0:T(8,128)(2,1)S(1)} copy-done((bf16[512,512]{1,0:T(8,128)(2,1)S(1)}, bf16[512,512]{1,0:T(8,128)(2,1)}, u32[]{:S(2)}) %copy-start.5) | copy-done | bytes 524312
  1.2 0.9 %copy-done.8 = bf16[2,256,255]{1,0,2:T(2,128)(2,1)S(1)} copy-done((bf16[2,256,255]{1,0,2:T(2,128)(2,1)S(1)}, bf16[2,256,255]{1,0,2:T(2,128)(2,1)}, u32[]{:S(2)}) %copy-start.8) | copy-done | bytes 261144
  2.2 0.0 copy-done.2
  2.2 0.0 copy-done.1
  2.2 0.0 copy-done.6
  2.2 0.0 copy-start.3
  2.3 0.2 shard_map.92.pack.after
  2.5 0.0 copy-start
  2.5 0.0 copy-start.4
  2.5 2.7 %collective-permute-start.2 = (bf16[912,1024]{1,0:T(8,128)(2,1)S(1)}, bf16[912,1024]{1,0:T(8,128)(2,1)S(1)}, u32[]{:S(2)}, u32[]{:S(2)}) collective-permute-start(bf16[912,1024]{1,0:T(8,128)(2,1)S(1)} %shard_map.92.pack.after), channel_id=1, source_target_pairs={{0,1},{1,0},{2,3},{3,2},{4,5},{5,4},{6,7},{7,6},{8,9},{9,8},{10,11... | collective-permute-start | bytes 5603336 | tf_op jit(solution)/shard_map/ppermute | solution.py:363
  5.3 0.0 copy-done.3
  5.3 0.2 shard_map.95.late
  5.5 1.9 %collective-permute-start.3 = (bf16[1024,1024]{1,0:T(8,128)(2,1)S(1)}, bf16[1024,1024]{1,0:T(8,128)(2,1)S(1)}, u32[]{:S(2)}, u32[]{:S(2)}) collective-permute-start(bf16[1024,1024]{1,0:T(8,128)(2,1)S(1)} %shard_map.95.late), channel_id=1, source_target_pairs={{0,1},{1,0},{2,3},{3,2},{4,5},{5,4},{6,7},{7,6},{8,9},{9,8},{10,11... | collective-permute-start | bytes 6291464 | tf_op jit(solution)/shard_map/ppermute | solution.py:369
  7.4 8.5 %collective-permute-start = (bf16[512,256]{1,0:T(8,128)(2,1)S(1)}, bf16[512,256]{1,0:T(8,128)(2,1)S(1)}, u32[]{:S(2)}, u32[]{:S(2)}) collective-permute-start(bf16[512,256]{1,0:T(8,128)(2,1)S(1)} %get-tuple-element.19.inner), channel_id=1, source_target_pairs={{0,2},{2,4},{4,6},{6,8},{8,10},{10,12},{12,14},{14,16},{16,18},{18... | collective-permute-start | bytes 786440 | tf_op jit(solution)/shard_map/ppermute | solution.py:354
  15.9 1.9 %collective-permute-start.1 = (bf16[512,256]{1,0:T(8,128)(2,1)S(1)}, bf16[512,256]{1,0:T(8,128)(2,1)S(1)}, u32[]{:S(2)}, u32[]{:S(2)}) collective-permute-start(bf16[512,256]{1,0:T(8,128)(2,1)S(1)} %get-tuple-element.20.outer), channel_id=1, source_target_pairs={{1,2},{3,4},{5,6},{7,8},{9,10},{11,12},{13,14},{15,16},{17,18},{19... | collective-permute-start | bytes 786440 | tf_op jit(solution)/shard_map/ppermute | solution.py:353
  17.9 0.5 %shard_map.93 = (f32[2,256,512]{2,1,0:T(8,128)S(1)}, f32[2,1024,128]{2,1,0:T(8,128)S(1)}) custom-call(f32[2,1024]{1,0:T(2,128)S(1)} %copy-done.4, bf16[912,1024]{1,0:T(8,128)(2,1)S(1)} %shard_map.92.pack.after, bf16[2048,512]{1,0:T(8,128)(2,1)S(1)} %copy-done), custom_call_target="tpu_custom_call" | custom-call | flops 1000000000 | bytes 4000000 | tf_op jit(solution)/shard_map/pallas_call | solution.py:326
  18.3 0.9 %collective-permute-done.halo_own = bf16[512,256]{1,0:T(8,128)(2,1)S(1)} collective-permute-done((bf16[512,256]{1,0:T(8,128)(2,1)S(1)}, bf16[512,256]{1,0:T(8,128)(2,1)S(1)}, u32[]{:S(2)}, u32[]{:S(2)}) %collective-permute-start) | collective-permute-done | bytes 262176 | tf_op jit(solution)/shard_map/ppermute | solution.py:354
  19.2 4.7 %collective-permute-done.1.halo_other = bf16[512,256]{1,0:T(8,128)(2,1)S(1)} collective-permute-done((bf16[512,256]{1,0:T(8,128)(2,1)S(1)}, bf16[512,256]{1,0:T(8,128)(2,1)S(1)}, u32[]{:S(2)}, u32[]{:S(2)}) %collective-permute-start.1) | collective-permute-done | bytes 262176 | tf_op jit(solution)/shard_map/ppermute | solution.py:353
  23.9 0.0 collective-permute-done.2.pack2
  23.9 5.1 %shard_map.94 = (bf16[1024,768]{1,0:T(8,128)(2,1)S(1)}, bf16[2,512,256]{2,1,0:T(8,128)(2,1)S(1)}) custom-call(f32[2,256,512]{2,1,0:T(8,128)S(1)} %get-tuple-element.21.bins, f32[2,1024,128]{2,1,0:T(8,128)S(1)} %get-tuple-element.22.gains, bf16[512,256]{1,0:T(8,128)(2,1)S(1)} %get-tuple-element.19.inner, bf16[512,256]{1,0:T(8,128)(2,1)S(1)} %get-tuple-element.20.outer, ...), custom_call_target="tpu_custom_call" | custom-call | flops 4000000000 | bytes 4000000 | tf_op jit(solution)/shard_map/pallas_call | solution.py:326
  29.0 0.0 collective-permute-done.3.late2
  29.0 4.1 %shard_map.96 = (bf16[512,256]{1,0:T(8,128)(2,1)S(1)}, bf16[512,256]{1,0:T(8,128)(2,1)S(1)}) custom-call(bf16[1024,768]{1,0:T(8,128)(2,1)S(1)} %get-tuple-element.23.xw, bf16[2,512,256]{2,1,0:T(8,128)(2,1)S(1)} %get-tuple-element.24.act, f32[2,256,512]{2,1,0:T(8,128)S(1)} %get-tuple-element.21.bins, f32[2,1024,128]{2,1,0:T(8,128)S(1)} %get-tuple-element.22.gains, ...), custom_call_target="tpu_custom_call" | custom-call | flops 3000000000 | bytes 4000000 | tf_op jit(solution)/shard_map/pallas_call | solution.py:326
  33.1 2.3 %all-gather = bf16[1024,256]{1,0:T(8,128)(2,1)S(1)} all-gather(bf16[512,256]{1,0:T(8,128)(2,1)S(1)} %get-tuple-element.26), channel_id=2, replica_groups=mesh['sp'=256,'tp'=2] {'tp'}, dimensions={0}, use_global_device_ids=true | all-gather | bytes 786432 | tf_op jit(solution)/shard_map/all_gather | solution.py:402
  35.5 0.9 %shard_map.97 = bf16[512,512]{1,0:T(8,128)(2,1)} custom-call(bf16[512,256]{1,0:T(8,128)(2,1)S(1)} %get-tuple-element.25.keep, bf16[2,512,256]{2,1,0:T(8,128)(2,1)S(1)} %bitcast.9), custom_call_target="tpu_custom_call" | custom-call | flops 100000000 | bytes 4000000 | tf_op jit(solution)/shard_map/pallas_call | solution.py:326
  (12 shorter events, 0.1 us)
Async XLA Ops:
  0.0 2.2 %copy-start.2 = (bf16[2,256,1024]{2,1,0:T(8,128)(2,1)S(1)}, bf16[2,256,1024]{2,1,0:T(8,128)(2,1)}, u32[]{:S(2)}) copy-start(bf16[2,256,1024]{2,1,0:T(8,128)(2,1)} %wg.3) | copy-start | bytes 3145732
  0.0 2.2 %copy-start.1 = (bf16[2,256,1024]{2,1,0:T(8,128)(2,1)S(1)}, bf16[2,256,1024]{2,1,0:T(8,128)(2,1)}, u32[]{:S(2)}) copy-start(bf16[2,256,1024]{2,1,0:T(8,128)(2,1)} %wv.3) | copy-start | bytes 3145732
  0.0 1.2 %copy-start.5 = (bf16[512,512]{1,0:T(8,128)(2,1)S(1)}, bf16[512,512]{1,0:T(8,128)(2,1)}, u32[]{:S(2)}) copy-start(bf16[512,512]{1,0:T(8,128)(2,1)} %stream.1) | copy-start | bytes 1572868
  1.2 0.9 %copy-start.8 = (bf16[2,256,255]{1,0,2:T(2,128)(2,1)S(1)}, bf16[2,256,255]{1,0,2:T(2,128)(2,1)}, u32[]{:S(2)}) copy-start(bf16[2,256,255]{1,0,2:T(2,128)(2,1)} %param.13) | copy-start | bytes 783364
  1.2 1.0 %copy-start.6 = (f32[2,256]{1,0:T(2,128)S(1)}, f32[2,256]{1,0:T(2,128)}, u32[]{:S(2)}) copy-start(f32[2,256]{1,0:T(2,128)} %ggain.1) | copy-start | bytes 6148
  1.2 1.0 %copy-start.7 = (f32[2,256]{1,0:T(2,128)S(1)}, f32[2,256]{1,0:T(2,128)}, u32[]{:S(2)}) copy-start(f32[2,256]{1,0:T(2,128)} %gshift.1) | copy-start | bytes 6148
  2.2 3.0 %copy-start.3 = (bf16[2,512,512]{2,1,0:T(8,128)(2,1)S(1)}, bf16[2,512,512]{2,1,0:T(8,128)(2,1)}, u32[]{:S(2)}) copy-start(bf16[2,512,512]{2,1,0:T(8,128)(2,1)} %wo.1) | copy-start | bytes 3145732
  2.5 15.3 %copy-start = (bf16[2048,512]{1,0:T(8,128)(2,1)S(1)}, bf16[2048,512]{1,0:T(8,128)(2,1)}, u32[]{:S(2)}) copy-start(bf16[2048,512]{1,0:T(8,128)(2,1)} %constant.2.clone.table) | copy-start | bytes 6291460
  2.5 15.3 %copy-start.4 = (f32[2,1024]{1,0:T(2,128)S(1)}, f32[2,1024]{1,0:T(2,128)}, u32[]{:S(2)}) copy-start(f32[2,1024]{1,0:T(2,128)} %gain.1) | copy-start | bytes 24580
  2.5 21.4 %collective-permute-start.2 = (bf16[912,1024]{1,0:T(8,128)(2,1)S(1)}, bf16[912,1024]{1,0:T(8,128)(2,1)S(1)}, u32[]{:S(2)}, u32[]{:S(2)}) collective-permute-start(bf16[912,1024]{1,0:T(8,128)(2,1)S(1)} %shard_map.92.pack.after), channel_id=1, source_target_pairs={{0,1},{1,0},{2,3},{3,2},{4,5},{5,4},{6,7},{7,6},{8,9},{9,8},{10,11... | collective-permute-start | bytes 5603336 | tf_op jit(solution)/shard_map/ppermute | solution.py:363
  5.5 23.5 %collective-permute-start.3 = (bf16[1024,1024]{1,0:T(8,128)(2,1)S(1)}, bf16[1024,1024]{1,0:T(8,128)(2,1)S(1)}, u32[]{:S(2)}, u32[]{:S(2)}) collective-permute-start(bf16[1024,1024]{1,0:T(8,128)(2,1)S(1)} %shard_map.95.late), channel_id=1, source_target_pairs={{0,1},{1,0},{2,3},{3,2},{4,5},{5,4},{6,7},{7,6},{8,9},{9,8},{10,11... | collective-permute-start | bytes 6291464 | tf_op jit(solution)/shard_map/ppermute | solution.py:369
  7.4 11.8 %collective-permute-start = (bf16[512,256]{1,0:T(8,128)(2,1)S(1)}, bf16[512,256]{1,0:T(8,128)(2,1)S(1)}, u32[]{:S(2)}, u32[]{:S(2)}) collective-permute-start(bf16[512,256]{1,0:T(8,128)(2,1)S(1)} %get-tuple-element.19.inner), channel_id=1, source_target_pairs={{0,2},{2,4},{4,6},{6,8},{8,10},{10,12},{12,14},{14,16},{16,18},{18... | collective-permute-start | bytes 786440 | tf_op jit(solution)/shard_map/ppermute | solution.py:354
  15.9 8.0 %collective-permute-start.1 = (bf16[512,256]{1,0:T(8,128)(2,1)S(1)}, bf16[512,256]{1,0:T(8,128)(2,1)S(1)}, u32[]{:S(2)}, u32[]{:S(2)}) collective-permute-start(bf16[512,256]{1,0:T(8,128)(2,1)S(1)} %get-tuple-element.20.outer), channel_id=1, source_target_pairs={{1,2},{3,4},{5,6},{7,8},{9,10},{11,12},{13,14},{15,16},{17,18},{19... | collective-permute-start | bytes 786440 | tf_op jit(solution)/shard_map/ppermute | solution.py:353

commit v5 on v4

--- a/solution.py
+++ b/solution.py
@@ -107,25 +107,43 @@
     return dot(taps, table[:256]) + dot(taps, table[256:512])
 
 
-def filter_norm(piece_of, bins, gcols, table, target):
-    for chunk in range(2):
-        piece = piece_of(slice(chunk * 256, (chunk + 1) * 256))
-        freq = dot(piece, table[512:1024]) + dot(piece, table[1024:1536])
+def filter_norm(pieces, bins, gcols, table, targets):
+    units = [(p, c, t) for p, t in zip(pieces, targets) for c in range(2)]
+
+    def forward(unit):
+        piece = unit[0](slice(unit[1] * 256, (unit[1] + 1) * 256))
+        return dot(piece, table[512:1024]) + dot(piece, table[1024:1536])
+
+    def spectrum(unit, freq):
         re, im = freq[:, :BINS], freq[:, BINS:]
-        tap_re, tap_im = bins[chunk][:, :BINS], bins[chunk][:, BINS:]
+        tap_re, tap_im = bins[unit[1]][:, :BINS], bins[unit[1]][:, BINS:]
         prod = jnp.concatenate([re * tap_re - im * tap_im, re * tap_im + im * tap_re], 1)
         high = prod.astype(jnp.bfloat16)
-        low = (prod - high.astype(jnp.float32)).astype(jnp.bfloat16)
+        return high, (prod - high.astype(jnp.float32)).astype(jnp.bfloat16)
+
+    def back(high, low):
         ih, il = table[1536:2048, :KEPT], table[1536:2048, KEPT:]
-        filtered = dot(high, ih) + dot(low, ih) + dot(high, il)
+        return dot(high, ih) + dot(low, ih) + dot(high, il)
+
+    def normalize(unit, filtered):
         for g in range(2):
             v = filtered[g * 128 : (g + 1) * 128]
-            c = slice(chunk * 256 + g * 128, chunk * 256 + (g + 1) * 128)
+            c = slice(unit[1] * 256 + g * 128, unit[1] * 256 + (g + 1) * 128)
             centred = v - jnp.mean(v, axis=0, keepdims=True)
             var = jnp.mean(centred * centred, axis=0, keepdims=True)
             scaled = centred * lax.rsqrt(var + LN_EPS)
             scaled = scaled * wide(gcols[0, c]) + wide(gcols[1, c])
-            target[c, :] = (scaled * sigmoid(scaled)).astype(jnp.bfloat16)
+            unit[2][c, :] = (scaled * sigmoid(scaled)).astype(jnp.bfloat16)
+
+    freq, before = forward(units[0]), None
+    for i, unit in enumerate(units):
+        following = forward(units[i + 1]) if i + 1 < len(units) else None
+        terms = spectrum(unit, freq)
+        filtered = back(*terms)
+        if before is not None:
+            normalize(*before)
+        freq, before = following, (unit, filtered)
+    normalize(*before)
 
 
 def group_columns(packs, layer, gcols):
@@ -209,8 +227,7 @@
         return lambda r: jnp.concatenate([gated[r, stored(b, me)], gated[r, stored(b + 1, me)]], 1)
 
     own = bins[0], bins2[...]
-    for b in range(2):
-        filter_norm(piece(b), own, gcols, table, act.at[b])
+    filter_norm([piece(0), piece(1)], own, gcols, table, [act.at[0], act.at[1]])
 
 
 def second_kernel(
@@ -252,7 +269,7 @@
             r = slice(chunk * 256, (chunk + 1) * 256)
             cols = slice(tile * HALF, (tile + 1) * HALF)
             gated[r, cols] = project_tile(source, normed2.at[tile], me)
-    filter_norm(lambda r: gated[r, :], (bins[1], bins2[...]), gcols, table, act2)
+    filter_norm([lambda r: gated[r, :]], (bins[1], bins2[...]), gcols, table, [act2])
     cols = slice(FIRST, FIRST + KEPT)
     for half, (source, out) in enumerate(((late, keep), (late2, send))):
         for part in range(2):

time: 36.5 us -> 35.6 us (0.975)
  Pallas kernels: 11 us -> 10.1 us
    pallas_call x7, Pallas kernels: 11 us -> 10.1 us  [call(): pl.pallas_call(kernel, out_shape=outs, in_specs=specs, out_specs=[vmem] *...]
  transfers between devices with their start and end apart: 4 -> 4, of which waited for: 2 -> 2; matrix products, arithmetic and copies ran while one was open for 0% -> 0% of each run, Pallas kernels for 16% -> 15%
where the time goes in v5:
time: 35.6 us; the launch traced here: 35.4 us
  starting transfers between devices  15 us (42%)
  Pallas kernels  10.1 us (28%)
  waiting for transfers between devices  5.58 us (16%)
  blocking collectives  2.31 us (6%)
  local copies, waits for them, and re-layouts  2.18 us (6%)
    pallas_call x7, Pallas kernels, call(): pl.pallas_call(kernel, out_shape=outs, in_specs=specs, out_specs=[vmem] *...  10.1 us
    ppermute x1, starting transfers between devices, body(): halo_own = lax.ppermute(inner, both, along)  8.49 us
    ppermute x1, waiting for transfers between devices, body(): halo_other = lax.ppermute(outer, both, outward)  4.69 us
    ppermute x1, starting transfers between devices, body(): pack2 = lax.ppermute(pack, both, partner)  2.72 us
    all_gather x1, blocking collectives, body(): swapped = lax.all_gather(send, 'tp', axis=0)  2.31 us
    unnamed x18, local copies, waits for them, and re-layouts  2.13 us
    ppermute x1, starting transfers between devices, body(): late2 = lax.ppermute(late, both, partner)  1.92 us
    ppermute x1, starting transfers between devices, body(): halo_other = lax.ppermute(outer, both, outward)  1.92 us
  transfers between devices with their start and end apart: 4, of which 2 were waited for; matrix products, arithmetic and copies ran while one was open for 0% of the time, Pallas kernels for 15%

profile of v5, /device:TPU:385, one launch (start us, length us, event | category | flops | bytes accessed | tf_op | source)
XLA Modules:
  0.0 35.4 jit_solution(1177801150074272632)
XLA Ops:
  0.0 1.2 %copy-done.5 = bf16[512,512]{1,0:T(8,128)(2,1)S(1)} copy-done((bf16[512,512]{1,0:T(8,128)(2,1)S(1)}, bf16[512,512]{1,0:T(8,128)(2,1)}, u32[]{:S(2)}) %copy-start.5) | copy-done | bytes 524312
  1.2 0.9 %copy-done.8 = bf16[2,256,255]{1,0,2:T(2,128)(2,1)S(1)} copy-done((bf16[2,256,255]{1,0,2:T(2,128)(2,1)S(1)}, bf16[2,256,255]{1,0,2:T(2,128)(2,1)}, u32[]{:S(2)}) %copy-start.8) | copy-done | bytes 261144
  2.2 0.0 copy-done.2
  2.2 0.0 copy-done.1
  2.2 0.0 copy-done.6
  2.2 0.0 copy-start.3
  2.3 0.2 shard_map.92.pack.after
  2.5 0.0 copy-start
  2.5 0.0 copy-start.4
  2.5 2.7 %collective-permute-start.2 = (bf16[912,1024]{1,0:T(8,128)(2,1)S(1)}, bf16[912,1024]{1,0:T(8,128)(2,1)S(1)}, u32[]{:S(2)}, u32[]{:S(2)}) collective-permute-start(bf16[912,1024]{1,0:T(8,128)(2,1)S(1)} %shard_map.92.pack.after), channel_id=1, source_target_pairs={{0,1},{1,0},{2,3},{3,2},{4,5},{5,4},{6,7},{7,6},{8,9},{9,8},{10,11... | collective-permute-start | bytes 5603336 | tf_op jit(solution)/shard_map/ppermute | solution.py:380
  5.3 0.0 copy-done.3
  5.3 0.2 shard_map.95.late
  5.5 1.9 %collective-permute-start.3 = (bf16[1024,1024]{1,0:T(8,128)(2,1)S(1)}, bf16[1024,1024]{1,0:T(8,128)(2,1)S(1)}, u32[]{:S(2)}, u32[]{:S(2)}) collective-permute-start(bf16[1024,1024]{1,0:T(8,128)(2,1)S(1)} %shard_map.95.late), channel_id=1, source_target_pairs={{0,1},{1,0},{2,3},{3,2},{4,5},{5,4},{6,7},{7,6},{8,9},{9,8},{10,11... | collective-permute-start | bytes 6291464 | tf_op jit(solution)/shard_map/ppermute | solution.py:386
  7.4 8.5 %collective-permute-start = (bf16[512,256]{1,0:T(8,128)(2,1)S(1)}, bf16[512,256]{1,0:T(8,128)(2,1)S(1)}, u32[]{:S(2)}, u32[]{:S(2)}) collective-permute-start(bf16[512,256]{1,0:T(8,128)(2,1)S(1)} %get-tuple-element.19.inner), channel_id=1, source_target_pairs={{0,2},{2,4},{4,6},{6,8},{8,10},{10,12},{12,14},{14,16},{16,18},{18... | collective-permute-start | bytes 786440 | tf_op jit(solution)/shard_map/ppermute | solution.py:371
  15.9 1.9 %collective-permute-start.1 = (bf16[512,256]{1,0:T(8,128)(2,1)S(1)}, bf16[512,256]{1,0:T(8,128)(2,1)S(1)}, u32[]{:S(2)}, u32[]{:S(2)}) collective-permute-start(bf16[512,256]{1,0:T(8,128)(2,1)S(1)} %get-tuple-element.20.outer), channel_id=1, source_target_pairs={{1,2},{3,4},{5,6},{7,8},{9,10},{11,12},{13,14},{15,16},{17,18},{19... | collective-permute-start | bytes 786440 | tf_op jit(solution)/shard_map/ppermute | solution.py:370
  17.9 0.5 %shard_map.93 = (f32[2,256,512]{2,1,0:T(8,128)S(1)}, f32[2,1024,128]{2,1,0:T(8,128)S(1)}) custom-call(f32[2,1024]{1,0:T(2,128)S(1)} %copy-done.4, bf16[912,1024]{1,0:T(8,128)(2,1)S(1)} %shard_map.92.pack.after, bf16[2048,512]{1,0:T(8,128)(2,1)S(1)} %copy-done), custom_call_target="tpu_custom_call" | custom-call | flops 1000000000 | bytes 4000000 | tf_op jit(solution)/shard_map/pallas_call | solution.py:343
  18.3 0.9 %collective-permute-done.halo_own = bf16[512,256]{1,0:T(8,128)(2,1)S(1)} collective-permute-done((bf16[512,256]{1,0:T(8,128)(2,1)S(1)}, bf16[512,256]{1,0:T(8,128)(2,1)S(1)}, u32[]{:S(2)}, u32[]{:S(2)}) %collective-permute-start) | collective-permute-done | bytes 262176 | tf_op jit(solution)/shard_map/ppermute | solution.py:371
  19.2 4.7 %collective-permute-done.1.halo_other = bf16[512,256]{1,0:T(8,128)(2,1)S(1)} collective-permute-done((bf16[512,256]{1,0:T(8,128)(2,1)S(1)}, bf16[512,256]{1,0:T(8,128)(2,1)S(1)}, u32[]{:S(2)}, u32[]{:S(2)}) %collective-permute-start.1) | collective-permute-done | bytes 262176 | tf_op jit(solution)/shard_map/ppermute | solution.py:370
  23.9 0.0 collective-permute-done.2.pack2
  23.9 4.7 %shard_map.94 = (bf16[1024,768]{1,0:T(8,128)(2,1)S(1)}, bf16[2,512,256]{2,1,0:T(8,128)(2,1)S(1)}) custom-call(f32[2,256,512]{2,1,0:T(8,128)S(1)} %get-tuple-element.21.bins, f32[2,1024,128]{2,1,0:T(8,128)S(1)} %get-tuple-element.22.gains, bf16[512,256]{1,0:T(8,128)(2,1)S(1)} %get-tuple-element.19.inner, bf16[512,256]{1,0:T(8,128)(2,1)S(1)} %get-tuple-element.20.outer, ...), custom_call_target="tpu_custom_call" | custom-call | flops 4000000000 | bytes 4000000 | tf_op jit(solution)/shard_map/pallas_call | solution.py:343
  28.6 0.0 collective-permute-done.3.late2
  28.6 3.6 %shard_map.96 = (bf16[512,256]{1,0:T(8,128)(2,1)S(1)}, bf16[512,256]{1,0:T(8,128)(2,1)S(1)}) custom-call(bf16[1024,768]{1,0:T(8,128)(2,1)S(1)} %get-tuple-element.23.xw, bf16[2,512,256]{2,1,0:T(8,128)(2,1)S(1)} %get-tuple-element.24.act, f32[2,256,512]{2,1,0:T(8,128)S(1)} %get-tuple-element.21.bins, f32[2,1024,128]{2,1,0:T(8,128)S(1)} %get-tuple-element.22.gains, ...), custom_call_target="tpu_custom_call" | custom-call | flops 3000000000 | bytes 4000000 | tf_op jit(solution)/shard_map/pallas_call | solution.py:343
  32.2 2.3 %all-gather = bf16[1024,256]{1,0:T(8,128)(2,1)S(1)} all-gather(bf16[512,256]{1,0:T(8,128)(2,1)S(1)} %get-tuple-element.26), channel_id=2, replica_groups=mesh['sp'=256,'tp'=2] {'tp'}, dimensions={0}, use_global_device_ids=true | all-gather | bytes 786432 | tf_op jit(solution)/shard_map/all_gather | solution.py:419
  34.5 0.9 %shard_map.97 = bf16[512,512]{1,0:T(8,128)(2,1)} custom-call(bf16[512,256]{1,0:T(8,128)(2,1)S(1)} %get-tuple-element.25.keep, bf16[2,512,256]{2,1,0:T(8,128)(2,1)S(1)} %bitcast.9), custom_call_target="tpu_custom_call" | custom-call | flops 100000000 | bytes 4000000 | tf_op jit(solution)/shard_map/pallas_call | solution.py:343
  (12 shorter events, 0.1 us)
Async XLA Ops:
  0.0 2.2 %copy-start.2 = (bf16[2,256,1024]{2,1,0:T(8,128)(2,1)S(1)}, bf16[2,256,1024]{2,1,0:T(8,128)(2,1)}, u32[]{:S(2)}) copy-start(bf16[2,256,1024]{2,1,0:T(8,128)(2,1)} %wg.3) | copy-start | bytes 3145732
  0.0 2.2 %copy-start.1 = (bf16[2,256,1024]{2,1,0:T(8,128)(2,1)S(1)}, bf16[2,256,1024]{2,1,0:T(8,128)(2,1)}, u32[]{:S(2)}) copy-start(bf16[2,256,1024]{2,1,0:T(8,128)(2,1)} %wv.3) | copy-start | bytes 3145732
  0.0 1.2 %copy-start.5 = (bf16[512,512]{1,0:T(8,128)(2,1)S(1)}, bf16[512,512]{1,0:T(8,128)(2,1)}, u32[]{:S(2)}) copy-start(bf16[512,512]{1,0:T(8,128)(2,1)} %stream.1) | copy-start | bytes 1572868
  1.2 0.9 %copy-start.8 = (bf16[2,256,255]{1,0,2:T(2,128)(2,1)S(1)}, bf16[2,256,255]{1,0,2:T(2,128)(2,1)}, u32[]{:S(2)}) copy-start(bf16[2,256,255]{1,0,2:T(2,128)(2,1)} %param.13) | copy-start | bytes 783364
  1.2 1.0 %copy-start.6 = (f32[2,256]{1,0:T(2,128)S(1)}, f32[2,256]{1,0:T(2,128)}, u32[]{:S(2)}) copy-start(f32[2,256]{1,0:T(2,128)} %ggain.1) | copy-start | bytes 6148
  1.2 1.0 %copy-start.7 = (f32[2,256]{1,0:T(2,128)S(1)}, f32[2,256]{1,0:T(2,128)}, u32[]{:S(2)}) copy-start(f32[2,256]{1,0:T(2,128)} %gshift.1) | copy-start | bytes 6148
  2.2 3.0 %copy-start.3 = (bf16[2,512,512]{2,1,0:T(8,128)(2,1)S(1)}, bf16[2,512,512]{2,1,0:T(8,128)(2,1)}, u32[]{:S(2)}) copy-start(bf16[2,512,512]{2,1,0:T(8,128)(2,1)} %wo.1) | copy-start | bytes 3145732
  2.5 15.3 %copy-start = (bf16[2048,512]{1,0:T(8,128)(2,1)S(1)}, bf16[2048,512]{1,0:T(8,128)(2,1)}, u32[]{:S(2)}) copy-start(bf16[2048,512]{1,0:T(8,128)(2,1)} %constant.2.clone.table) | copy-start | bytes 6291460
  2.5 15.3 %copy-start.4 = (f32[2,1024]{1,0:T(2,128)S(1)}, f32[2,1024]{1,0:T(2,128)}, u32[]{:S(2)}) copy-start(f32[2,1024]{1,0:T(2,128)} %gain.1) | copy-start | bytes 24580
  2.5 21.4 %collective-permute-start.2 = (bf16[912,1024]{1,0:T(8,128)(2,1)S(1)}, bf16[912,1024]{1,0:T(8,128)(2,1)S(1)}, u32[]{:S(2)}, u32[]{:S(2)}) collective-permute-start(bf16[912,1024]{1,0:T(8,128)(2,1)S(1)} %shard_map.92.pack.after), channel_id=1, source_target_pairs={{0,1},{1,0},{2,3},{3,2},{4,5},{5,4},{6,7},{7,6},{8,9},{9,8},{10,11... | collective-permute-start | bytes 5603336 | tf_op jit(solution)/shard_map/ppermute | solution.py:380
  5.5 23.1 %collective-permute-start.3 = (bf16[1024,1024]{1,0:T(8,128)(2,1)S(1)}, bf16[1024,1024]{1,0:T(8,128)(2,1)S(1)}, u32[]{:S(2)}, u32[]{:S(2)}) collective-permute-start(bf16[1024,1024]{1,0:T(8,128)(2,1)S(1)} %shard_map.95.late), channel_id=1, source_target_pairs={{0,1},{1,0},{2,3},{3,2},{4,5},{5,4},{6,7},{7,6},{8,9},{9,8},{10,11... | collective-permute-start | bytes 6291464 | tf_op jit(solution)/shard_map/ppermute | solution.py:386
  7.4 11.8 %collective-permute-start = (bf16[512,256]{1,0:T(8,128)(2,1)S(1)}, bf16[512,256]{1,0:T(8,128)(2,1)S(1)}, u32[]{:S(2)}, u32[]{:S(2)}) collective-permute-start(bf16[512,256]{1,0:T(8,128)(2,1)S(1)} %get-tuple-element.19.inner), channel_id=1, source_target_pairs={{0,2},{2,4},{4,6},{6,8},{8,10},{10,12},{12,14},{14,16},{16,18},{18... | collective-permute-start | bytes 786440 | tf_op jit(solution)/shard_map/ppermute | solution.py:371
  15.9 8.0 %collective-permute-start.1 = (bf16[512,256]{1,0:T(8,128)(2,1)S(1)}, bf16[512,256]{1,0:T(8,128)(2,1)S(1)}, u32[]{:S(2)}, u32[]{:S(2)}) collective-permute-start(bf16[512,256]{1,0:T(8,128)(2,1)S(1)} %get-tuple-element.20.outer), channel_id=1, source_target_pairs={{1,2},{3,4},{5,6},{7,8},{9,10},{11,12},{13,14},{15,16},{17,18},{19... | collective-permute-start | bytes 786440 | tf_op jit(solution)/shard_map/ppermute | solution.py:370
